TPU v7x, 32 devices: a whole 2x2x4 slice. The times are simulated.
32 devices in a mesh: sp: 8 (over z, y), tp: 4 (over x, core).
Axes of the slice: x: 2, y: 2, z: 4, core: 2. Of those that a mesh axis runs over, the one named last changes fastest.
Arguments:
- inputs: bfloat16 [2, 1024, 2048], P(None, 'sp'), may hold values from -6 to 6
- norm_gain: float32 [2048], replicated, may hold values from 0.1 to 1.9
- query_weight: bfloat16 [2048, 1024], P('sp', 'tp'), may hold values from -0.125 to 0.125
- key_weight: bfloat16 [2048, 256], P('sp', 'tp'), may hold values from -0.125 to 0.125
- value_weight: bfloat16 [2048, 256], P('sp', 'tp'), may hold values from -0.125 to 0.125
- query_gain: float32 [64], replicated, may hold values from 0.1 to 24
- key_gain: float32 [64], replicated, may hold values from 0.1 to 1.9
- forget_cache: float32 [2, 16, 1024], P(None, 'tp'), may hold values from -104 to 0, as said below
- rec_in_weight: bfloat16 [2048, 1024], P('sp', 'tp'), may hold values from -0.125 to 0.125
- rec_gate_weight: bfloat16 [2048, 1024], P('sp', 'tp'), may hold values from -0.125 to 0.125
- conv_weight: bfloat16 [4, 1024], P(None, 'tp'), may hold values from -3 to 3
- decay_gate_weight: bfloat16 [16, 64, 64], P('tp'), may hold values from -0.75 to 0.75
- input_gate_weight: bfloat16 [16, 64, 64], P('tp'), may hold values from -0.75 to 0.75
- decay_param: float32 [1024], P('tp'), may hold values from 4 to 16
- decay_extra: float32 [2, 1024, 1024], P(None, 'sp', 'tp'), may hold values from -2 to 0
- attn_out_gain: float32 [1024], P('tp'), may hold values from 0.1 to 1.9
- rec_out_gain: float32 [1024], P('tp'), may hold values from 0.1 to 1.9
- out_att_weight: bfloat16 [1024, 2048], P('tp'), may hold values from -0.125 to 0.125
- out_rec_weight: bfloat16 [1024, 2048], P('tp'), may hold values from -0.125 to 0.125
Outputs:
- mixed: bfloat16 [2, 1024, 2048], P(None, 'sp', 'tp')
Inputs may be any that keep to these rules, and one draw needn't show every extreme that they name: `forget_cache`: Non-increasing along the positions of each sequence and head.
All inputs are finite; a program needn't handle non-finite values.
Results may differ from a plain program's by a relative error of at most 0.012.
The roundings to bfloat16 on the way count: a program that leaves them out, or rounds other values in their place, can miss the bound.
Values may be sent and summed in bfloat16 or wider, within the bound.
A program may use at most 128 MiB of HBM per device.

v0:
```python
import functools

import jax
import jax.numpy as jnp
from jax import lax
from jax.experimental import pallas as pl
from jax.experimental.pallas import tpu as pltpu
from jax.sharding import PartitionSpec as P

LRU_CONST = 8.0
EPS = 1e-06
F32 = jnp.float32
BF16 = jnp.bfloat16
MESH = pl.DeviceIdType.MESH


def group_rms(values, gain, width):
    parts = []
    for start in range(0, values.shape[1], width):
        part = values[:, start : start + width]
        scale = lax.rsqrt(jnp.mean(part * part, axis=-1, keepdims=True) + EPS)
        parts.append(part * scale)
    return jnp.concatenate(parts, axis=1) * gain


def one_minus_exp(y):
    series = y * (1 + y / 2 * (1 + y / 3 * (1 + y / 4 * (1 + y / 5 * (1 + y / 6 * (1 + y / 7))))))
    return -jnp.where(y > -0.4, series, jnp.exp(y) - 1.0)


def softplus(x):
    u = jnp.exp(-jnp.abs(x))
    s = u / (2.0 + u)
    q = s * s
    series = 1.0 / 17
    for odd in (15, 13, 11, 9, 7, 5, 3, 1):
        series = series * q + 1.0 / odd
    return jnp.maximum(x, 0.0) + 2.0 * s * series


def sigmoid(x):
    return 1.0 / (1.0 + jnp.exp(-x))


def gelu(x):
    return 0.5 * x * (1.0 + jnp.tanh(0.7978845608028654 * (x + 0.044715 * x * x * x)))


def dot(a, b):
    return jnp.dot(a, b, preferred_element_type=F32)


def kernel(
    dims,
    x_ref, norm_ref, wq_ref, wk_ref, wv_ref, qg_ref, kg_ref, fc_ref, wr_ref, wg_ref, cw_ref,
    dgw_ref, igw_ref, dp_ref, de_ref, ag_ref, rg_ref, oa_ref, or_ref,
    out_ref,
    normed, kvw, rw, qw, gw, kv_all, rin, halo, st_all, halves, sums, parts, got,
    zs, zr, fs, fr, hs, hr, ss, sr, ps, pr, qs, qr,
):
    n, nt, seqs, span, head_dim, block, length = dims
    rows = seqs * span
    no, nto = n // 2, nt // 2
    me = lax.axis_index("sp")
    outer, inner = lax.div(me, 2), lax.rem(me, 2)
    mate = outer * 2 + (1 - inner)
    tme = lax.axis_index("tp")
    touter, tinner = lax.div(tme, 2), lax.rem(tme, 2)
    tmate = touter * 2 + (1 - tinner)
    kr = wq_ref.shape[0]
    kvc = wk_ref.shape[1]
    att_local = wq_ref.shape[1] // head_dim
    kv_local = kvc // head_dim
    hg = att_local // kv_local
    taps = cw_ref.shape[0]

    def to_outer(d):
        return lax.rem(outer + d, no) * 2 + inner

    def from_outer(d):
        return lax.rem(outer + no - d, no) * 2 + inner

    barrier = pltpu.get_barrier_semaphore()
    for d in range(1, n):
        pl.semaphore_signal(barrier, inc=1, device_id={"sp": lax.rem(me + d, n)}, device_id_type=MESH)
    for d in range(1, nt):
        pl.semaphore_signal(barrier, inc=1, device_id={"tp": lax.rem(tme + d, nt)}, device_id_type=MESH)

    def slot(ref, who):
        return ref.at[pl.ds(pl.multiple_of(who * kr, kr), kr), :]

    own_rows = pl.ds(pl.multiple_of(me * kr, kr), kr)
    kvw[own_rows, :] = jnp.concatenate([wk_ref[...], wv_ref[...]], axis=1)
    rw[own_rows, :] = wr_ref[...]
    qw[own_rows, :] = wq_ref[...]
    gw[own_rows, :] = wg_ref[...]
    pl.semaphore_wait(barrier, n - 1 + nt - 1)

    buffers = (kvw, rw, qw, gw, kv_all)
    sources = (None, wr_ref, wq_ref, wg_ref, None)

    def place(c, who):
        return kv_all.at[who] if c == 4 else slot(buffers[c], who)

    def origin(c):
        return place(c, me) if sources[c] is None else sources[c]

    def outward(c, d, who, src):
        return pltpu.make_async_remote_copy(
            src_ref=src, dst_ref=place(c, who), send_sem=zs.at[c, d - 1], recv_sem=zr.at[c, d - 1],
            device_id={"sp": to_outer(d)}, device_id_type=MESH,
        )

    def across(c, d, who, src):
        return pltpu.make_async_remote_copy(
            src_ref=src, dst_ref=place(c, who), send_sem=fs.at[c, d], recv_sem=fr.at[c, d],
            device_id={"sp": mate}, device_id_type=MESH,
        )

    def send_own(c):
        for d in range(1, no):
            outward(c, d, me, origin(c)).start()
        across(c, 0, me, origin(c)).start()

    def forward(c):
        for d in range(1, no):
            who = from_outer(d)
            outward(c, d, who, place(c, who)).wait_recv()
            across(c, d, who, place(c, who)).start()

    def finish(c):
        for d in range(no):
            who = lax.rem(outer + no - d, no) * 2 + (1 - inner)
            across(c, d, who, place(c, who)).wait_recv()

    def drain(c):
        for d in range(1, no):
            outward(c, d, me, origin(c)).wait_send()
        across(c, 0, me, origin(c)).wait_send()
        for d in range(1, no):
            who = from_outer(d)
            across(c, d, who, place(c, who)).wait_send()

    send_own(0)
    send_own(1)
    send_own(2)

    x = x_ref[...].astype(F32)
    scale = lax.rsqrt(jnp.mean(x * x, axis=-1, keepdims=True) + EPS)
    normed[...] = (x * scale * norm_ref[...]).astype(BF16)

    forward(0)
    forward(1)
    finish(0)
    kv = dot(normed[...], kvw[...])
    keys = jnp.concatenate(
        [group_rms(kv[:, g * head_dim : (g + 1) * head_dim], kg_ref[...], head_dim) for g in range(kv_local)], axis=1
    )
    kv_all[me] = jnp.concatenate([keys, kv[:, kvc:]], axis=1).astype(BF16)
    send_own(4)

    finish(1)
    rec = dot(normed[...], rw[...]).astype(BF16).astype(F32)
    nxt, prv = lax.rem(me + 1, n), lax.rem(me + n - 1, n)
    for b in range(seqs):
        rin[b, pl.ds(8, span), :] = rec[b * span : (b + 1) * span]
    for b in range(seqs):
        halo[0, pl.ds(b * 8, 8), :] = rin[b, pl.ds(span, 8), :]
    halo_copy = pltpu.make_async_remote_copy(
        src_ref=halo.at[0], dst_ref=halo.at[1], send_sem=hs, recv_sem=hr,
        device_id={"sp": nxt}, device_id_type=MESH,
    )
    halo_copy.start()
    send_own(3)

    forward(2)
    forward(4)

    halo_copy.wait()
    first = me == 0
    for b in range(seqs):
        edge = halo[1, pl.ds(b * 8, 8), :]
        rin[b, pl.ds(0, 8), :] = jnp.where(first, jnp.zeros_like(edge), edge)
    convs = []
    for b in range(seqs):
        conv = jnp.zeros((span, rw.shape[1]), F32)
        for tap in range(taps):
            conv = conv + rin[b, pl.ds(8 - (taps - 1) + tap, span), :] * cw_ref[pl.ds(tap, 1), :]
        convs.append(conv)
    conv = jnp.concatenate(convs, axis=0).astype(BF16)
    nb, lb = dgw_ref.shape[0], dgw_ref.shape[1]
    gate_decay = jnp.concatenate([dot(conv[:, i * lb : (i + 1) * lb], dgw_ref[i]) for i in range(nb)], axis=1)
    gate_input = jnp.concatenate([dot(conv[:, i * lb : (i + 1) * lb], igw_ref[i]) for i in range(nb)], axis=1)
    log_decay = -LRU_CONST * sigmoid(gate_decay) * softplus(-dp_ref[...]) + de_ref[...]
    state = jnp.sqrt(one_minus_exp(2.0 * log_decay)) * sigmoid(gate_input) * conv.astype(F32)
    decay = jnp.exp(log_decay)
    time = lax.rem(lax.broadcasted_iota(jnp.int32, state.shape, 0), span)
    shift = 1
    while shift < span:
        seen = time >= shift
        state = state + decay * jnp.where(seen, pltpu.roll(state, shift, 0), 0.0)
        decay = decay * jnp.where(seen, pltpu.roll(decay, shift, 0), 1.0)
        shift *= 2
    ends = [decay[(b + 1) * span - 1 : (b + 1) * span] for b in range(seqs)]
    ends += [state[(b + 1) * span - 1 : (b + 1) * span] for b in range(seqs)]
    for i, row in enumerate(ends):
        st_all[me, pl.ds(i, 1), :] = row
    def state_copy(d, who):
        return pltpu.make_async_remote_copy(
            src_ref=st_all.at[who], dst_ref=st_all.at[who], send_sem=ss.at[d - 1], recv_sem=sr.at[d - 1],
            device_id={"sp": lax.rem(me + d, n)}, device_id_type=MESH,
        )

    for d in range(1, n):
        state_copy(d, me).start()

    finish(2)
    scaling = head_dim ** (-0.5)
    query = dot(normed[...], qw[...])
    queries = [
        (group_rms(query[:, h * head_dim : (h + 1) * head_dim], qg_ref[...], head_dim).astype(BF16) * scaling).astype(BF16)
        for h in range(att_local)
    ]
    finish(4)
    shards = block // span
    first_pos = me * span
    query_pos = first_pos + lax.broadcasted_iota(jnp.int32, (span, block), 0)
    key_off = lax.broadcasted_iota(jnp.int32, (span, block), 1)
    needed = lax.div(first_pos + span + block - 1, block)
    attended = []
    for b in range(seqs):
        heads = []
        for h in range(att_local):
            g = h // hg
            q = queries[h][b * span : (b + 1) * span]

            def step(j, carried, q=q, b=b, h=h, g=g):
                top, total, accum = carried
                kvb = kv_all[pl.ds(j * shards, shards), pl.ds(b * span, span), :].reshape(block, 2 * kvc)
                kb = kvb[:, g * head_dim : (g + 1) * head_dim]
                vb = kvb[:, kvc + g * head_dim : kvc + (g + 1) * head_dim]
                s = lax.dot_general(q, kb, (((1,), (1,)), ((), ())), preferred_element_type=F32)
                s = s - fc_ref[b, pl.ds(h, 1), pl.ds(pl.multiple_of(j * block, block), block)]
                s = jnp.where(query_pos >= key_off + j * block, s, -jnp.inf)
                new_top = jnp.maximum(top, jnp.max(s, axis=-1, keepdims=True))
                w = jnp.exp(s - new_top)
                fade = jnp.exp(top - new_top)
                total = total * fade + jnp.sum(w, axis=-1, keepdims=True)
                return new_top, total, accum * fade + dot(w.astype(BF16), vb)

            start = (jnp.full((span, 1), -1e30, F32), jnp.zeros((span, 1), F32), jnp.zeros((span, head_dim), F32))
            if length == block:
                top, total, accum = step(0, start)
            else:
                top, total, accum = lax.fori_loop(0, needed, step, start)
            value = accum / total
            value = value * lax.rsqrt(jnp.mean(value * value, axis=-1, keepdims=True) + EPS)
            heads.append(value)
        attended.append(jnp.concatenate(heads, axis=1))
    halves[0] = (jnp.concatenate(attended, axis=0) * ag_ref[...]).astype(BF16)

    forward(3)
    for d in range(1, n):
        state_copy(d, lax.rem(me + n - d, n)).wait_recv()

    def enter(j, e):
        block_state = st_all[j]
        return block_state[0:seqs] * e + block_state[seqs : 2 * seqs]

    entering = lax.fori_loop(0, me, enter, jnp.zeros((seqs, rw.shape[1]), F32))
    whole_state = jnp.concatenate(
        [
            state[b * span : (b + 1) * span] + decay[b * span : (b + 1) * span] * entering[b : b + 1]
            for b in range(seqs)
        ],
        axis=0,
    )
    finish(3)
    gated = whole_state * gelu(dot(normed[...], gw[...]))
    halves[1] = group_rms(gated, rg_ref[...], lb).astype(BF16)

    cols = out_ref.shape[1]

    def piece(who):
        span_cols = pl.ds(pl.multiple_of(who * cols, cols), cols)
        return dot(halves[0], oa_ref[:, span_cols]) + dot(halves[1], or_ref[:, span_cols])

    def to_mate(s):
        return pltpu.make_async_remote_copy(
            src_ref=sums.at[s], dst_ref=parts.at[s], send_sem=ps.at[s], recv_sem=pr.at[s],
            device_id={"tp": tmate}, device_id_type=MESH,
        )

    def to_far(d):
        return pltpu.make_async_remote_copy(
            src_ref=sums.at[nto + d - 1], dst_ref=got.at[d - 1], send_sem=qs.at[d - 1], recv_sem=qr.at[d - 1],
            device_id={"tp": lax.rem(touter + d, nto) * 2 + tinner}, device_id_type=MESH,
        )

    for s in list(range(1, nto)) + [0]:
        sums[s] = piece(lax.rem(touter + s, nto) * 2 + (1 - tinner)).astype(BF16)
        to_mate(s).start()
    for d in range(1, nto):
        mine = piece(lax.rem(touter + d, nto) * 2 + tinner)
        to_mate(d).wait_recv()
        sums[nto + d - 1] = (mine + parts[d].astype(F32)).astype(BF16)
        to_far(d).start()
    mine = piece(tme)
    to_mate(0).wait_recv()
    mine = mine + parts[0].astype(F32)
    for d in range(1, nto):
        to_far(d).wait_recv()
        mine = mine + got[d - 1].astype(F32)
    out_ref[...] = mine.astype(BF16)

    for c in range(5):
        drain(c)
    for d in range(1, n):
        state_copy(d, me).wait_send()
    for s in range(nto):
        to_mate(s).wait_send()
    for d in range(1, nto):
        to_far(d).wait_send()


def body(
    n, nt,
    inputs, norm_gain, query_weight, key_weight, value_weight, query_gain, key_gain, forget_cache,
    rec_in_weight, rec_gate_weight, conv_weight, decay_gate_weight, input_gate_weight, decay_param,
    decay_extra, attn_out_gain, rec_out_gain, out_att_weight, out_rec_weight,
):
    seqs, span, width = inputs.shape
    rows = seqs * span
    head_dim = query_gain.shape[0]
    length = forget_cache.shape[2]
    channels = rec_in_weight.shape[1]
    qc, kvc = query_weight.shape[1], key_weight.shape[1]
    cols = out_att_weight.shape[1] // nt
    block = span
    while block * 2 <= 1024 and length % (block * 2) == 0:
        block *= 2
    no, nto = n // 2, nt // 2
    dma = pltpu.SemaphoreType.DMA
    vmem = pl.BlockSpec(memory_space=pltpu.VMEM)
    out = pl.pallas_call(
        functools.partial(kernel, (n, nt, seqs, span, head_dim, block, length)),
        out_shape=jax.ShapeDtypeStruct((rows, cols), BF16),
        in_specs=[vmem] * 19,
        out_specs=vmem,
        scratch_shapes=[
            pltpu.VMEM((rows, width), BF16),
            pltpu.VMEM((width, 2 * kvc), BF16),
            pltpu.VMEM((width, channels), BF16),
            pltpu.VMEM((width, qc), BF16),
            pltpu.VMEM((width, channels), BF16),
            pltpu.VMEM((n, rows, 2 * kvc), BF16),
            pltpu.VMEM((seqs, span + 8, channels), F32),
            pltpu.VMEM((2, seqs * 8, channels), F32),
            pltpu.VMEM((n, -(-2 * seqs // 8) * 8, channels), F32),
            pltpu.VMEM((2, rows, channels), BF16),
            pltpu.VMEM((2 * nto, rows, cols), BF16),
            pltpu.VMEM((nto, rows, cols), BF16),
            pltpu.VMEM((nto, rows, cols), BF16),
            dma((5, no)), dma((5, no)), dma((5, no)), dma((5, no)),
            dma, dma, dma((n,)), dma((n,)),
            dma((nto,)), dma((nto,)), dma((nto,)), dma((nto,)),
        ],
        compiler_params=pltpu.CompilerParams(
            collective_id=0, has_side_effects=True, vmem_limit_bytes=60 * 1024 * 1024
        ),
    )(
        inputs.reshape(rows, width), norm_gain.reshape(1, width), query_weight, key_weight, value_weight,
        query_gain.reshape(1, head_dim), key_gain.reshape(1, head_dim), forget_cache,
        rec_in_weight, rec_gate_weight, conv_weight.astype(F32), decay_gate_weight, input_gate_weight,
        decay_param.reshape(1, channels), decay_extra.reshape(rows, channels),
        attn_out_gain.reshape(1, qc), rec_out_gain.reshape(1, channels), out_att_weight, out_rec_weight,
    )
    return out.reshape(seqs, span, cols)


def solution(mesh):
    return jax.shard_map(
        functools.partial(body, mesh.shape["sp"], mesh.shape["tp"]),
        mesh=mesh,
        in_specs=(
            P(None, "sp", None), P(), P("sp", "tp"), P("sp", "tp"), P("sp", "tp"), P(), P(),
            P(None, "tp", None), P("sp", "tp"), P("sp", "tp"), P(None, "tp"), P("tp", None, None),
            P("tp", None, None), P("tp"), P(None, "sp", "tp"), P("tp"), P("tp"), P("tp", None), P("tp", None),
        ),
        out_specs=P(None, "sp", "tp"),
        check_vma=False,
    )
```

profile of v0, /device:TPU:1, one launch (start us, length us, event | category | flops | bytes accessed | tf_op | source)
XLA Modules:
  0.0 84.0 jit_solution(5291823098604318668)
XLA Ops:
  0.0 0.0 copy-start.1
  0.0 0.7 copy-done.1
  0.7 0.6 convert_element_type.3.cw_ref
  1.3 0.0 copy-start
  1.3 1.5 %copy.20.wk_ref = bf16[256,64]{1,0:T(8,128)(2,1)} copy(bf16[256,64]{0,1:T(8,128)(2,1)} %param.22) | data formatting | bytes 65536 | tf_op args[3]
  2.8 0.0 copy-done
  2.8 0.7 copy.21.wv_ref
  3.5 78.8 %shard_map.181 = bf16[256,512]{1,0:T(8,128)(2,1)} custom-call(bf16[256,2048]{1,0:T(8,128)(2,1)} %bitcast.10, f32[1,2048]{1,0:T(1,128)} %bitcast.12, bf16[256,256]{1,0:T(8,128)(2,1)} %wq_ref.1, bf16[256,64]{1,0:T(8,128)(2,1)} %copy.20.wk_ref, bf16[256,64]{1,0:T(8,128)(2,1)} %copy.21.wv_ref, f32[1,64]{1,0:T(1,128)} %bitcast.16, f32[1,64]{1,0:T(1,128)} %bitcast.17, ...), custom_call_target="tpu_custom_call" | custom-call | tf_op jit(solution)/shard_map/pallas_call | solution.py:345
  82.3 1.7 %copy.23 = bf16[2,128,512]{2,1,0:T(8,128)(2,1)} copy(bf16[2,128,512]{2,1,0:T(8,128)(2,1)} %bitcast.9) | data formatting | bytes 524288
Async XLA Ops:
  0.0 0.7 copy-start.1
  1.3 1.5 %copy-start = (bf16[256,64]{0,1:T(8,128)(2,1)S(1)}, bf16[256,64]{0,1:T(8,128)(2,1)}, u32[]{:S(2)}) copy-start(bf16[256,64]{0,1:T(8,128)(2,1)} %param.23) | copy-start | bytes 98308
where the time goes:
time: 84.6 us; the launch traced here: 84 us
  Pallas kernels  78.8 us (93%)
  local copies, waits for them, and re-layouts  4.59 us (5%)
    pallas_call x1, Pallas kernels, body(): pl.pallas_call(functools.partial(kernel, (n, nt, seqs, span, head_dim, bl...  78.8 us
    unnamed x7, local copies, waits for them, and re-layouts  4.59 us

commit v1 on v0

v1 whole, which is shorter than its diff:
```python
import functools

import jax
import jax.numpy as jnp
from jax import lax
from jax.experimental import pallas as pl
from jax.experimental.pallas import tpu as pltpu
from jax.sharding import PartitionSpec as P

LRU_CONST = 8.0
EPS = 1e-06
F32 = jnp.float32
BF16 = jnp.bfloat16
MESH = pl.DeviceIdType.MESH


def group_rms(values, gain, width):
    parts = []
    for start in range(0, values.shape[1], width):
        part = values[:, start : start + width]
        scale = lax.rsqrt(jnp.mean(part * part, axis=-1, keepdims=True) + EPS)
        parts.append(part * scale)
    return jnp.concatenate(parts, axis=1) * gain


def one_minus_exp(y):
    series = y * (1 + y / 2 * (1 + y / 3 * (1 + y / 4 * (1 + y / 5 * (1 + y / 6 * (1 + y / 7))))))
    return -jnp.where(y > -0.4, series, jnp.exp(y) - 1.0)


def softplus(x):
    u = jnp.exp(-jnp.abs(x))
    s = u / (2.0 + u)
    q = s * s
    series = 1.0 / 17
    for odd in (15, 13, 11, 9, 7, 5, 3, 1):
        series = series * q + 1.0 / odd
    return jnp.maximum(x, 0.0) + 2.0 * s * series


def sigmoid(x):
    return 1.0 / (1.0 + jnp.exp(-x))


def gelu(x):
    return 0.5 * x * (1.0 + jnp.tanh(0.7978845608028654 * (x + 0.044715 * x * x * x)))


def dot(a, b):
    return jnp.dot(a, b, preferred_element_type=F32)


def kernel(
    dims,
    x_ref, norm_ref, wq_ref, wk_ref, wv_ref, qg_ref, kg_ref, fc_ref, wr_ref, wg_ref, cw_ref,
    dgw_ref, igw_ref, dp_ref, de_ref, ag_ref, rg_ref, oa_ref, or_ref,
    out_ref,
    xall, xsend, kvw, rw, qw, gw, kv_all, deg, rin, halo, st_all, act, halves, sums, parts, got,
    zs, zr, fs, fr, xas, xar, xbs, xbr, xcs, xcr, xds, xdr, des, der, kvs, kvr, hs, hr, ss, sr,
    acs, acr, ps, pr, qs, qr,
):
    n, nt, span, head_dim, flip = dims
    no, nto, ng = n // 2, nt // 2, n // 4
    me = lax.axis_index("sp")
    outer, inner = lax.div(me, 2), lax.rem(me, 2)
    grp, mem = lax.div(outer, 2), lax.rem(outer, 2)
    opp, omem = 1 - inner, 1 - mem
    mate = outer * 2 + opp
    pair = (grp * 2 + omem) * 2 + inner
    cross = (grp * 2 + omem) * 2 + opp
    tme = lax.axis_index("tp")
    touter, tinner = lax.div(tme, 2), lax.rem(tme, 2)
    tmate = touter * 2 + (1 - tinner)
    kr, channels = wq_ref.shape
    kvc = wk_ref.shape[0 if flip else 1]
    width = x_ref.shape[1]
    half = channels // 2
    quarter = width // nt
    heads = half // head_dim
    taps = cw_ref.shape[0]
    gp = 4 * span

    def rows_of(i, size):
        return pl.ds(pl.multiple_of(i * size, size), size)

    def to_outer(d):
        return lax.rem(outer + d, no)

    def from_outer(d):
        return lax.rem(outer + no - d, no)

    def copy(src, dst, send, recv, **where):
        return pltpu.make_async_remote_copy(
            src_ref=src, dst_ref=dst, send_sem=send, recv_sem=recv, device_id=where, device_id_type=MESH
        )

    barrier = pltpu.get_barrier_semaphore()
    for d in range(1, n):
        pl.semaphore_signal(barrier, inc=1, device_id={"sp": lax.rem(me + d, n)}, device_id_type=MESH)
    for d in range(1, nt):
        pl.semaphore_signal(barrier, inc=1, device_id={"tp": lax.rem(tme + d, nt)}, device_id_type=MESH)

    mine_block, mate_block = mem * 2 + inner, mem * 2 + opp
    pair_block, cross_block = omem * 2 + inner, omem * 2 + opp
    my_half, my_rows = rows_of(mem, half), rows_of(me, kr)
    my_cols = rows_of(tme, quarter)

    if flip:
        kvw[0:kvc, my_rows] = wk_ref[...]
        kvw[kvc : 2 * kvc, my_rows] = wv_ref[...]
    else:
        kvw[my_rows, :] = jnp.concatenate([wk_ref[...], wv_ref[...]], axis=1)

    def scale_rows(seq):
        x = x_ref[rows_of(seq, span), :].astype(F32)
        return lax.rsqrt(jnp.mean(x * x, axis=-1, keepdims=True) + EPS)

    xsend[...] = (
        x_ref[rows_of(opp, span), my_cols].astype(F32) * scale_rows(opp) * norm_ref[:, my_cols]
    ).astype(BF16)
    xall[mine_block] = (x_ref[rows_of(inner, span), :].astype(F32) * scale_rows(inner) * norm_ref[...]).astype(BF16)
    pl.semaphore_wait(barrier, n - 1 + nt - 1)

    weights = (None, wr_ref, wq_ref, wg_ref)
    buffers = (kvw, rw, qw, gw)

    def place(c, who):
        return kvw.at[:, rows_of(who, kr)] if c == 0 and flip else buffers[c].at[rows_of(who, kr), :]

    def origin(c, member):
        return place(0, me) if c == 0 else weights[c].at[:, rows_of(member, half)]

    def outward(c, d):
        to = to_outer(d)
        return copy(origin(c, lax.rem(to, 2)), place(c, me), zs.at[c, d - 1], zr.at[c, d - 1], sp=to * 2 + inner)

    def inward(c, d):
        who = from_outer(d) * 2 + inner
        return copy(place(c, who), place(c, who), zs.at[c, d - 1], zr.at[c, d - 1], sp=mate)

    def across(c, d, who, src=None):
        return copy(place(c, who) if src is None else src, place(c, who), fs.at[c, d], fr.at[c, d], sp=mate)

    def send_own(c):
        for d in range(1, no):
            outward(c, d).start()
        across(c, 0, me, origin(c, mem)).start()

    def forward(c):
        for d in range(1, no):
            inward(c, d).wait_recv()
            across(c, d, from_outer(d) * 2 + inner).start()

    def finish(c):
        for d in range(no):
            across(c, d, from_outer(d) * 2 + opp).wait_recv()

    def drain(c):
        for d in range(1, no):
            outward(c, d).wait_send()
        across(c, 0, me, origin(c, mem)).wait_send()
        for d in range(1, no):
            across(c, d, from_outer(d) * 2 + inner).wait_send()

    def piece_of(block, who=None):
        return xall.at[block, :, my_cols if who is None else rows_of(who, quarter)]

    to_mate_x = copy(xsend, piece_of(mine_block), xas, xar, sp=mate)
    to_pair_x = [
        copy(piece_of(mine_block), piece_of(mine_block), xbs.at[0], xbr.at[0], sp=pair),
        copy(piece_of(mate_block), piece_of(mate_block), xbs.at[1], xbr.at[1], sp=pair),
    ]
    shared = (mate_block, pair_block, cross_block)

    def to_far_x(k, d):
        far = lax.rem(touter + d, nto) * 2 + tinner
        return copy(piece_of(shared[k]), piece_of(shared[k]), xcs.at[k, d - 1], xcr.at[k, d - 1], tp=far)

    def to_core_x(k, d):
        ref = piece_of(shared[k], lax.rem(touter + nto - d, nto) * 2 + tinner)
        return copy(ref, ref, xds.at[k, d], xdr.at[k, d], tp=tmate)

    def spread(k):
        for d in range(1, nto):
            to_far_x(k, d).start()
        to_core_x(k, 0).start()

    def extra(i):
        to, seq, member = ((mate, opp, mem), (pair, inner, omem), (cross, opp, omem))[i]
        src = de_ref.at[rows_of(seq, span), rows_of(member, half)]
        return copy(src, deg.at[mine_block], des.at[i], der.at[i], sp=to)

    to_mate_x.start()
    to_pair_x[0].start()
    send_own(0)
    for i in range(3):
        extra(i).start()
    send_own(1)
    deg[mine_block] = de_ref[rows_of(inner, span), my_half]
    rw[my_rows, :] = wr_ref[:, my_half]
    qw[my_rows, :] = wq_ref[:, my_half]
    gw[my_rows, :] = wg_ref[:, my_half]

    to_mate_x.wait_recv()
    to_pair_x[1].start()
    spread(0)
    to_pair_x[0].wait_recv()
    spread(1)
    send_own(2)
    forward(0)
    to_pair_x[1].wait_recv()
    spread(2)
    send_own(3)
    for k in range(3):
        for d in range(1, nto):
            to_far_x(k, d).wait_recv()
            to_core_x(k, d).start()
    forward(1)
    for k in range(3):
        for d in range(nto):
            to_core_x(k, d).wait_recv()
    finish(0)

    def normed():
        return xall[...].reshape(gp, width)

    kv = lax.dot_general(normed(), kvw[...], (((1,), (1 if flip else 0,)), ((), ())), preferred_element_type=F32)
    keys = group_rms(kv[:, :kvc], kg_ref[...], head_dim)
    kv_all[grp] = jnp.concatenate([keys, kv[:, kvc:]], axis=1).astype(BF16)

    def kv_copy(d, who):
        to = lax.rem(grp + d, ng) * 4 + mem * 2 + inner
        return copy(kv_all.at[who], kv_all.at[who], kvs.at[d - 1], kvr.at[d - 1], sp=to)

    def state_copy(d, who):
        to = lax.rem(grp + d, ng) * 4 + mem * 2 + inner
        return copy(st_all.at[who], st_all.at[who], ss.at[d - 1], sr.at[d - 1], sp=to)

    def later(make, act_on):
        for d in range(1, ng):
            @pl.when(grp + d < ng)
            def _(d=d):
                act_on(make(d, grp))

    def earlier(make):
        for d in range(1, ng):
            @pl.when(grp >= d)
            def _(d=d):
                make(d, lax.rem(grp + ng - d, ng)).wait_recv()

    later(kv_copy, lambda c: c.start())

    finish(1)
    rec = dot(normed(), rw[...]).astype(BF16).astype(F32)
    rin[pl.ds(8, gp), :] = rec
    halo[0] = rec[gp - 8 : gp]
    halo[1] = jnp.zeros_like(halo[1])
    halo_copy = copy(halo.at[0], halo.at[2], hs, hr, sp=lax.rem(grp + 1, ng) * 4 + mem * 2 + inner)

    @pl.when(grp + 1 < ng)
    def _():
        halo_copy.start()

    forward(2)
    finish(2)
    scaling = head_dim ** (-0.5)
    query = dot(normed(), qw[...])
    queries = [
        (group_rms(query[:, h * head_dim : (h + 1) * head_dim], qg_ref[...], head_dim).astype(BF16) * scaling).astype(BF16)
        for h in range(heads)
    ]

    @pl.when(grp > 0)
    def _():
        halo_copy.wait_recv()
        halo[1] = halo[2]

    for i, block in ((0, mate_block), (1, pair_block), (2, cross_block)):
        copy(deg.at[block], deg.at[block], des.at[i], der.at[i], sp=mate).wait_recv()
    rin[pl.ds(0, 8), :] = halo[1]
    cw = cw_ref[:, my_half].astype(F32)
    conv = jnp.zeros((gp, half), F32)
    for tap in range(taps):
        conv = conv + rin[pl.ds(8 - (taps - 1) + tap, gp), :] * cw[tap : tap + 1]
    conv = conv.astype(BF16)
    lb = dgw_ref.shape[1]
    nb = half // lb
    gate_decay = jnp.concatenate([dot(conv[:, i * lb : (i + 1) * lb], dgw_ref[mem * nb + i]) for i in range(nb)], axis=1)
    gate_input = jnp.concatenate([dot(conv[:, i * lb : (i + 1) * lb], igw_ref[mem * nb + i]) for i in range(nb)], axis=1)
    log_decay = -LRU_CONST * sigmoid(gate_decay) * softplus(-dp_ref[:, my_half]) + deg[...].reshape(gp, half)
    state = jnp.sqrt(one_minus_exp(2.0 * log_decay)) * sigmoid(gate_input) * conv.astype(F32)
    decay = jnp.exp(log_decay)
    time = lax.broadcasted_iota(jnp.int32, state.shape, 0)
    shift = 1
    while shift < gp:
        if shift < 8:
            seen = time >= shift
            state = state + decay * jnp.where(seen, pltpu.roll(state, shift, 0), 0.0)
            decay = decay * jnp.where(seen, pltpu.roll(decay, shift, 0), 1.0)
        else:
            moved = state[shift:] + decay[shift:] * state[: gp - shift]
            faded = decay[shift:] * decay[: gp - shift]
            state = jnp.concatenate([state[:shift], moved], axis=0)
            decay = jnp.concatenate([decay[:shift], faded], axis=0)
        shift *= 2
    st_all[grp, pl.ds(0, 1), :] = decay[gp - 1 : gp]
    st_all[grp, pl.ds(1, 1), :] = state[gp - 1 : gp]
    later(state_copy, lambda c: c.start())

    def attend(carried, q, kb, vb, fade_row, mask):
        top, total, accum = carried
        s = lax.dot_general(q, kb, (((1,), (1,)), ((), ())), preferred_element_type=F32) - fade_row
        if mask is not None:
            s = jnp.where(mask, s, -jnp.inf)
        new_top = jnp.maximum(top, jnp.max(s, axis=-1, keepdims=True))
        w = jnp.exp(s - new_top)
        fade = jnp.exp(top - new_top)
        total = total * fade + jnp.sum(w, axis=-1, keepdims=True)
        return new_top, total, accum * fade + dot(w.astype(BF16), vb)

    qb = gp // 2
    jobs = [(h, i) for h in range(heads) for i in range(2)]
    kv_own = kv_all[grp]
    carried = []
    for h, i in jobs:
        size = (i + 1) * qb
        kb, vb = kv_own[:size, :kvc], kv_own[:size, kvc:]
        fade_row = fc_ref[inner, pl.ds(mem * heads + h, 1), pl.ds(pl.multiple_of(grp * gp, gp), size)]
        mask = i * qb + lax.broadcasted_iota(jnp.int32, (qb, size), 0) >= lax.broadcasted_iota(jnp.int32, (qb, size), 1)
        start = (jnp.full((qb, 1), -1e30, F32), jnp.zeros((qb, 1), F32), jnp.zeros((qb, head_dim), F32))
        carried.append(attend(start, queries[h][i * qb : size], kb, vb, fade_row, mask))

    forward(3)
    earlier(kv_copy)

    def step(j, carried):
        result = []
        kb, vb = kv_all[j, :, :kvc], kv_all[j, :, kvc:]
        for (h, i), state_of in zip(jobs, carried):
            fade_row = fc_ref[inner, pl.ds(mem * heads + h, 1), pl.ds(pl.multiple_of(j * gp, gp), gp)]
            result.append(attend(state_of, queries[h][i * qb : (i + 1) * qb], kb, vb, fade_row, None))
        return tuple(result)

    carried = lax.fori_loop(0, grp, step, tuple(carried))
    columns = []
    for h in range(heads):
        pieces = []
        for (hh, i), (top, total, accum) in zip(jobs, carried):
            if hh == h:
                value = accum / total
                pieces.append(value * lax.rsqrt(jnp.mean(value * value, axis=-1, keepdims=True) + EPS))
        columns.append(jnp.concatenate(pieces, axis=0))

    def act_copy(a, i):
        to, block = ((mate, mate_block), (pair, pair_block), (cross, cross_block))[i]
        return copy(
            act.at[a, block], halves.at[a, rows_of(inner, span), my_half], acs.at[a, i], acr.at[a, i], sp=to
        )

    def act_from(a, i):
        seq, member = ((opp, mem), (inner, omem), (opp, omem))[i]
        ref = halves.at[a, rows_of(seq, span), rows_of(member, half)]
        return copy(ref, ref, acs.at[a, i], acr.at[a, i], sp=mate)

    def hand_out(a, values):
        act[a] = values.astype(BF16).reshape(4, span, half)
        for i in range(3):
            act_copy(a, i).start()
        halves[a, rows_of(inner, span), my_half] = act[a, mine_block]

    hand_out(0, jnp.concatenate(columns, axis=1) * ag_ref[:, my_half])

    earlier(state_copy)

    def enter(j, e):
        return st_all[j, pl.ds(0, 1), :] * e + st_all[j, pl.ds(1, 1), :]

    entering = lax.fori_loop(0, grp, enter, jnp.zeros((1, half), F32))
    whole_state = state + decay * entering
    finish(3)
    gated = whole_state * gelu(dot(normed(), gw[...]))
    hand_out(1, group_rms(gated, rg_ref[:, my_half], lb))
    for a in range(2):
        for i in range(3):
            act_from(a, i).wait_recv()

    cols = out_ref.shape[1]

    def piece(who):
        span_cols = pl.ds(pl.multiple_of(who * cols, cols), cols)
        return dot(halves[0], oa_ref[:, span_cols]) + dot(halves[1], or_ref[:, span_cols])

    def to_mate(s):
        return pltpu.make_async_remote_copy(
            src_ref=sums.at[s], dst_ref=parts.at[s], send_sem=ps.at[s], recv_sem=pr.at[s],
            device_id={"tp": tmate}, device_id_type=MESH,
        )

    def to_far(d):
        return pltpu.make_async_remote_copy(
            src_ref=sums.at[nto + d - 1], dst_ref=got.at[d - 1], send_sem=qs.at[d - 1], recv_sem=qr.at[d - 1],
            device_id={"tp": lax.rem(touter + d, nto) * 2 + tinner}, device_id_type=MESH,
        )

    for s in list(range(1, nto)) + [0]:
        sums[s] = piece(lax.rem(touter + s, nto) * 2 + (1 - tinner)).astype(BF16)
        to_mate(s).start()
    for d in range(1, nto):
        mine = piece(lax.rem(touter + d, nto) * 2 + tinner)
        to_mate(d).wait_recv()
        sums[nto + d - 1] = (mine + parts[d].astype(F32)).astype(BF16)
        to_far(d).start()
    mine = piece(tme)
    to_mate(0).wait_recv()
    mine = mine + parts[0].astype(F32)
    for d in range(1, nto):
        to_far(d).wait_recv()
        mine = mine + got[d - 1].astype(F32)
    out_ref[...] = mine.astype(BF16)

    for c in range(4):
        drain(c)
    to_mate_x.wait_send()
    for c in to_pair_x:
        c.wait_send()
    for k in range(3):
        extra(k).wait_send()
        for d in range(1, nto):
            to_far_x(k, d).wait_send()
        for d in range(nto):
            to_core_x(k, d).wait_send()
    later(kv_copy, lambda c: c.wait_send())
    later(state_copy, lambda c: c.wait_send())

    @pl.when(grp + 1 < ng)
    def _():
        halo_copy.wait_send()

    for a in range(2):
        for i in range(3):
            act_copy(a, i).wait_send()
    for s in range(nto):
        to_mate(s).wait_send()
    for d in range(1, nto):
        to_far(d).wait_send()


def body(
    n, nt,
    inputs, norm_gain, query_weight, key_weight, value_weight, query_gain, key_gain, forget_cache,
    rec_in_weight, rec_gate_weight, conv_weight, decay_gate_weight, input_gate_weight, decay_param,
    decay_extra, attn_out_gain, rec_out_gain, out_att_weight, out_rec_weight,
):
    seqs, span, width = inputs.shape
    assert seqs == 2 and n % 4 == 0 and nt % 2 == 0 and key_weight.shape[1] == query_gain.shape[0]
    rows = seqs * span
    head_dim = query_gain.shape[0]
    channels = rec_in_weight.shape[1]
    qc, kvc = query_weight.shape[1], key_weight.shape[1]
    half = channels // 2
    cols = out_att_weight.shape[1] // nt
    flip = query_weight.shape[0] % 128 == 0
    kv_weights = [w.T if flip else w for w in (key_weight, value_weight)]
    no, nto, ng = n // 2, nt // 2, n // 4
    dma = pltpu.SemaphoreType.DMA
    vmem = pl.BlockSpec(memory_space=pltpu.VMEM)
    out = pl.pallas_call(
        functools.partial(kernel, (n, nt, span, head_dim, flip)),
        out_shape=jax.ShapeDtypeStruct((rows, cols), BF16),
        in_specs=[vmem] * 19,
        out_specs=vmem,
        scratch_shapes=[
            pltpu.VMEM((4, span, width), BF16),
            pltpu.VMEM((span, width // nt), BF16),
            pltpu.VMEM((2 * kvc, width) if flip else (width, 2 * kvc), BF16),
            pltpu.VMEM((width, half), BF16),
            pltpu.VMEM((width, half), BF16),
            pltpu.VMEM((width, half), BF16),
            pltpu.VMEM((ng, 4 * span, 2 * kvc), BF16),
            pltpu.VMEM((4, span, half), F32),
            pltpu.VMEM((4 * span + 8, half), F32),
            pltpu.VMEM((3, 8, half), F32),
            pltpu.VMEM((ng, 8, half), F32),
            pltpu.VMEM((2, 4, span, half), BF16),
            pltpu.VMEM((2, rows, channels), BF16),
            pltpu.VMEM((2 * nto, rows, cols), BF16),
            pltpu.VMEM((nto, rows, cols), BF16),
            pltpu.VMEM((nto, rows, cols), BF16),
            dma((4, no)), dma((4, no)), dma((4, no)), dma((4, no)),
            dma, dma, dma((2,)), dma((2,)), dma((3, nto)), dma((3, nto)), dma((3, nto)), dma((3, nto)),
            dma((3,)), dma((3,)), dma((ng,)), dma((ng,)), dma, dma, dma((ng,)), dma((ng,)),
            dma((2, 3)), dma((2, 3)), dma((nto,)), dma((nto,)), dma((nto,)), dma((nto,)),
        ],
        compiler_params=pltpu.CompilerParams(
            collective_id=0, has_side_effects=True, vmem_limit_bytes=60 * 1024 * 1024
        ),
    )(
        inputs.reshape(rows, width), norm_gain.reshape(1, width), query_weight, *kv_weights,
        query_gain.reshape(1, head_dim), key_gain.reshape(1, head_dim), forget_cache,
        rec_in_weight, rec_gate_weight, conv_weight, decay_gate_weight, input_gate_weight,
        decay_param.reshape(1, channels), decay_extra.reshape(rows, channels),
        attn_out_gain.reshape(1, qc), rec_out_gain.reshape(1, channels), out_att_weight, out_rec_weight,
    )
    return out.reshape(seqs, span, cols)


def solution(mesh):
    return jax.shard_map(
        functools.partial(body, mesh.shape["sp"], mesh.shape["tp"]),
        mesh=mesh,
        in_specs=(
            P(None, "sp", None), P(), P("sp", "tp"), P("sp", "tp"), P("sp", "tp"), P(), P(),
            P(None, "tp", None), P("sp", "tp"), P("sp", "tp"), P(None, "tp"), P("tp", None, None),
            P("tp", None, None), P("tp"), P(None, "sp", "tp"), P("tp"), P("tp"), P("tp", None), P("tp", None),
        ),
        out_specs=P(None, "sp", "tp"),
        check_vma=False,
    )
```

time: 84.6 us -> 73 us (0.86)
  Pallas kernels: 78.8 us -> 70.6 us
  local copies, waits for them, and re-layouts: 4.59 us -> 1.67 us
    pallas_call x1, Pallas kernels: 78.8 us -> 70.6 us  [body(): pl.pallas_call(functools.partial(kernel, (n, nt, span, head_dim, flip)),...]
    unnamed x7 -> x1, local copies, waits for them, and re-layouts: 4.59 us -> 1.67 us
where the time goes in v1:
time: 73 us; the launch traced here: 72.2 us
  Pallas kernels  70.6 us (97%)
  local copies, waits for them, and re-layouts  1.67 us (2%)
    pallas_call x1, Pallas kernels, body(): pl.pallas_call(functools.partial(kernel, (n, nt, span, head_dim, flip)),...  70.6 us
    unnamed x1, local copies, waits for them, and re-layouts  1.67 us

profile of v1, /device:TPU:1, one launch (start us, length us, event | category | flops | bytes accessed | tf_op | source)
XLA Modules:
  0.0 72.2 jit_solution(13534987670690753178)
XLA Ops:
  0.0 70.6 %shard_map.181 = bf16[256,512]{1,0:T(8,128)(2,1)} custom-call(bf16[256,2048]{1,0:T(8,128)(2,1)} %bitcast.11, f32[1,2048]{1,0:T(1,128)} %bitcast.16, bf16[256,256]{1,0:T(8,128)(2,1)} %wq_ref.1, bf16[64,256]{1,0:T(8,128)(2,1)} %bitcast.14, bf16[64,256]{1,0:T(8,128)(2,1)} %bitcast.15, f32[1,64]{1,0:T(1,128)} %bitcast.20, f32[1,64]{1,0:T(1,128)} %bitcast.21, ...), custom_call_target="tpu_custom_call" | custom-call | tf_op jit(solution)/shard_map/pallas_call | solution.py:467
  70.6 1.7 %copy.21 = bf16[2,128,512]{2,1,0:T(8,128)(2,1)} copy(bf16[2,128,512]{2,1,0:T(8,128)(2,1)} %bitcast.12) | data formatting | bytes 524288

commit v2 on v1

--- a/solution.py
+++ b/solution.py
@@ -55,8 +55,8 @@
     x_ref, norm_ref, wq_ref, wk_ref, wv_ref, qg_ref, kg_ref, fc_ref, wr_ref, wg_ref, cw_ref,
     dgw_ref, igw_ref, dp_ref, de_ref, ag_ref, rg_ref, oa_ref, or_ref,
     out_ref,
-    xall, xsend, kvw, rw, qw, gw, kv_all, deg, rin, halo, st_all, act, halves, sums, parts, got,
-    zs, zr, fs, fr, xas, xar, xbs, xbr, xcs, xcr, xds, xdr, des, der, kvs, kvr, hs, hr, ss, sr,
+    xall, xsend, kvsrc, kvw, rw, qw, gw, kv_all, scanned, deg, rin, halo, st_all, act, halves, sums, parts, got,
+    zs, zr, fs, fr, xas, xar, xbs, xbr, xcs, xcr, xds, xdr, des, der, kvs, kvr, kps, kpr, hs, hr, ss, sr,
     acs, acr, ps, pr, qs, qr,
 ):
     n, nt, span, head_dim, flip = dims
@@ -83,11 +83,13 @@
     def rows_of(i, size):
         return pl.ds(pl.multiple_of(i * size, size), size)
 
-    def to_outer(d):
-        return lax.rem(outer + d, no)
-
-    def from_outer(d):
-        return lax.rem(outer + no - d, no)
+    def partner(d):
+        who, bit = 0, 1
+        while bit < no:
+            own = lax.rem(lax.div(outer, bit), 2)
+            who = who + bit * (1 - own if d & bit else own)
+            bit *= 2
+        return who
 
     def copy(src, dst, send, recv, **where):
         return pltpu.make_async_remote_copy(
@@ -105,11 +107,8 @@
     my_half, my_rows = rows_of(mem, half), rows_of(me, kr)
     my_cols = rows_of(tme, quarter)
 
-    if flip:
-        kvw[0:kvc, my_rows] = wk_ref[...]
-        kvw[kvc : 2 * kvc, my_rows] = wv_ref[...]
-    else:
-        kvw[my_rows, :] = jnp.concatenate([wk_ref[...], wv_ref[...]], axis=1)
+    kvsrc[0] = wk_ref[...]
+    kvsrc[1] = wv_ref[...]
 
     def scale_rows(seq):
         x = x_ref[rows_of(seq, span), :].astype(F32)
@@ -128,39 +127,41 @@
         return kvw.at[:, rows_of(who, kr)] if c == 0 and flip else buffers[c].at[rows_of(who, kr), :]
 
     def origin(c, member):
-        return place(0, me) if c == 0 else weights[c].at[:, rows_of(member, half)]
+        return kvsrc.at[member] if c == 0 else weights[c].at[:, rows_of(member, half)]
 
     def outward(c, d):
-        to = to_outer(d)
+        to = partner(d)
         return copy(origin(c, lax.rem(to, 2)), place(c, me), zs.at[c, d - 1], zr.at[c, d - 1], sp=to * 2 + inner)
 
     def inward(c, d):
-        who = from_outer(d) * 2 + inner
+        who = partner(d) * 2 + inner
         return copy(place(c, who), place(c, who), zs.at[c, d - 1], zr.at[c, d - 1], sp=mate)
 
     def across(c, d, who, src=None):
         return copy(place(c, who) if src is None else src, place(c, who), fs.at[c, d], fr.at[c, d], sp=mate)
 
-    def send_own(c):
+    def send_z(c):
         for d in range(1, no):
             outward(c, d).start()
+
+    def send_y(c):
         across(c, 0, me, origin(c, mem)).start()
 
-    def forward(c):
-        for d in range(1, no):
+    def forward(c, which=range(1, no)):
+        for d in which:
             inward(c, d).wait_recv()
-            across(c, d, from_outer(d) * 2 + inner).start()
+            across(c, d, partner(d) * 2 + inner).start()
 
     def finish(c):
         for d in range(no):
-            across(c, d, from_outer(d) * 2 + opp).wait_recv()
+            across(c, d, partner(d) * 2 + opp).wait_recv()
 
     def drain(c):
         for d in range(1, no):
             outward(c, d).wait_send()
         across(c, 0, me, origin(c, mem)).wait_send()
         for d in range(1, no):
-            across(c, d, from_outer(d) * 2 + inner).wait_send()
+            across(c, d, partner(d) * 2 + inner).wait_send()
 
     def piece_of(block, who=None):
         return xall.at[block, :, my_cols if who is None else rows_of(who, quarter)]
@@ -192,11 +193,14 @@
 
     to_mate_x.start()
     to_pair_x[0].start()
-    send_own(0)
-    for i in range(3):
-        extra(i).start()
-    send_own(1)
+    send_z(0)
+    for c in range(3):
+        send_y(c)
     deg[mine_block] = de_ref[rows_of(inner, span), my_half]
+    if flip:
+        kvw[:, my_rows] = kvsrc[mem]
+    else:
+        kvw[my_rows, :] = kvsrc[mem]
     rw[my_rows, :] = wr_ref[:, my_half]
     qw[my_rows, :] = wq_ref[:, my_half]
     gw[my_rows, :] = wg_ref[:, my_half]
@@ -204,18 +208,21 @@
     to_mate_x.wait_recv()
     to_pair_x[1].start()
     spread(0)
+    send_z(1)
     to_pair_x[0].wait_recv()
     spread(1)
-    send_own(2)
     forward(0)
+    send_y(3)
     to_pair_x[1].wait_recv()
     spread(2)
-    send_own(3)
+    send_z(2)
+    for i in range(3):
+        extra(i).start()
+    forward(1)
     for k in range(3):
         for d in range(1, nto):
             to_far_x(k, d).wait_recv()
             to_core_x(k, d).start()
-    forward(1)
     for k in range(3):
         for d in range(nto):
             to_core_x(k, d).wait_recv()
@@ -225,12 +232,16 @@
         return xall[...].reshape(gp, width)
 
     kv = lax.dot_general(normed(), kvw[...], (((1,), (1 if flip else 0,)), ((), ())), preferred_element_type=F32)
-    keys = group_rms(kv[:, :kvc], kg_ref[...], head_dim)
-    kv_all[grp] = jnp.concatenate([keys, kv[:, kvc:]], axis=1).astype(BF16)
+    kv = jnp.where(mem == 0, group_rms(kv, kg_ref[...], head_dim), kv).astype(BF16)
+    kv_all[mem, grp] = jnp.concatenate([kv[: gp // 2], kv[gp // 2 :]], axis=1)
 
     def kv_copy(d, who):
-        to = lax.rem(grp + d, ng) * 4 + mem * 2 + inner
-        return copy(kv_all.at[who], kv_all.at[who], kvs.at[d - 1], kvr.at[d - 1], sp=to)
+        to, ref = lax.rem(grp + d, ng) * 4 + mem * 2 + inner, kv_all.at[mem, who]
+        return copy(ref, ref, kvs.at[d - 1], kvr.at[d - 1], sp=to)
+
+    def kv_pair(d, member, who):
+        ref = kv_all.at[member, who]
+        return copy(ref, ref, kps.at[d], kpr.at[d], sp=pair)
 
     def state_copy(d, who):
         to = lax.rem(grp + d, ng) * 4 + mem * 2 + inner
@@ -248,6 +259,7 @@
             def _(d=d):
                 make(d, lax.rem(grp + ng - d, ng)).wait_recv()
 
+    kv_pair(0, mem, grp).start()
     later(kv_copy, lambda c: c.start())
 
     finish(1)
@@ -261,7 +273,48 @@
     def _():
         halo_copy.start()
 
+    send_z(3)
     forward(2)
+    lb = dgw_ref.shape[1]
+
+    def recur():
+        for i, block in ((0, mate_block), (1, pair_block), (2, cross_block)):
+            copy(deg.at[block], deg.at[block], des.at[i], der.at[i], sp=mate).wait_recv()
+        rin[pl.ds(0, 8), :] = halo[1]
+        cw = cw_ref[:, my_half].astype(F32)
+        conv = jnp.zeros((gp, half), F32)
+        for tap in range(taps):
+            conv = conv + rin[pl.ds(8 - (taps - 1) + tap, gp), :] * cw[tap : tap + 1]
+        conv = conv.astype(BF16)
+        nb = half // lb
+        gate_decay = jnp.concatenate([dot(conv[:, i * lb : (i + 1) * lb], dgw_ref[mem * nb + i]) for i in range(nb)], axis=1)
+        gate_input = jnp.concatenate([dot(conv[:, i * lb : (i + 1) * lb], igw_ref[mem * nb + i]) for i in range(nb)], axis=1)
+        log_decay = -LRU_CONST * sigmoid(gate_decay) * softplus(-dp_ref[:, my_half]) + deg[...].reshape(gp, half)
+        state = jnp.sqrt(one_minus_exp(2.0 * log_decay)) * sigmoid(gate_input) * conv.astype(F32)
+        decay = jnp.exp(log_decay)
+        time = lax.broadcasted_iota(jnp.int32, state.shape, 0)
+        shift = 1
+        while shift < gp:
+            if shift < 8:
+                seen = time >= shift
+                state = state + decay * jnp.where(seen, pltpu.roll(state, shift, 0), 0.0)
+                decay = decay * jnp.where(seen, pltpu.roll(decay, shift, 0), 1.0)
+            else:
+                moved = state[shift:] + decay[shift:] * state[: gp - shift]
+                faded = decay[shift:] * decay[: gp - shift]
+                state = jnp.concatenate([state[:shift], moved], axis=0)
+                decay = jnp.concatenate([decay[:shift], faded], axis=0)
+            shift *= 2
+        scanned[0] = decay
+        scanned[1] = state
+        st_all[grp, pl.ds(0, 1), :] = decay[gp - 1 : gp]
+        st_all[grp, pl.ds(1, 1), :] = state[gp - 1 : gp]
+        later(state_copy, lambda c: c.start())
+
+    @pl.when(grp == 0)
+    def _():
+        recur()
+
     finish(2)
     scaling = head_dim ** (-0.5)
     query = dot(normed(), qw[...])
@@ -270,43 +323,8 @@
         for h in range(heads)
     ]
 
-    @pl.when(grp > 0)
-    def _():
-        halo_copy.wait_recv()
-        halo[1] = halo[2]
-
-    for i, block in ((0, mate_block), (1, pair_block), (2, cross_block)):
-        copy(deg.at[block], deg.at[block], des.at[i], der.at[i], sp=mate).wait_recv()
-    rin[pl.ds(0, 8), :] = halo[1]
-    cw = cw_ref[:, my_half].astype(F32)
-    conv = jnp.zeros((gp, half), F32)
-    for tap in range(taps):
-        conv = conv + rin[pl.ds(8 - (taps - 1) + tap, gp), :] * cw[tap : tap + 1]
-    conv = conv.astype(BF16)
-    lb = dgw_ref.shape[1]
-    nb = half // lb
-    gate_decay = jnp.concatenate([dot(conv[:, i * lb : (i + 1) * lb], dgw_ref[mem * nb + i]) for i in range(nb)], axis=1)
-    gate_input = jnp.concatenate([dot(conv[:, i * lb : (i + 1) * lb], igw_ref[mem * nb + i]) for i in range(nb)], axis=1)
-    log_decay = -LRU_CONST * sigmoid(gate_decay) * softplus(-dp_ref[:, my_half]) + deg[...].reshape(gp, half)
-    state = jnp.sqrt(one_minus_exp(2.0 * log_decay)) * sigmoid(gate_input) * conv.astype(F32)
-    decay = jnp.exp(log_decay)
-    time = lax.broadcasted_iota(jnp.int32, state.shape, 0)
-    shift = 1
-    while shift < gp:
-        if shift < 8:
-            seen = time >= shift
-            state = state + decay * jnp.where(seen, pltpu.roll(state, shift, 0), 0.0)
-            decay = decay * jnp.where(seen, pltpu.roll(decay, shift, 0), 1.0)
-        else:
-            moved = state[shift:] + decay[shift:] * state[: gp - shift]
-            faded = decay[shift:] * decay[: gp - shift]
-            state = jnp.concatenate([state[:shift], moved], axis=0)
-            decay = jnp.concatenate([decay[:shift], faded], axis=0)
-        shift *= 2
-    st_all[grp, pl.ds(0, 1), :] = decay[gp - 1 : gp]
-    st_all[grp, pl.ds(1, 1), :] = state[gp - 1 : gp]
-    later(state_copy, lambda c: c.start())
-
+    forward(3, range(1, no - 1))
+    kv_pair(0, omem, grp).wait_recv()
     def attend(carried, q, kb, vb, fade_row, mask):
         top, total, accum = carried
         s = lax.dot_general(q, kb, (((1,), (1,)), ((), ())), preferred_element_type=F32) - fade_row
@@ -320,22 +338,38 @@
 
     qb = gp // 2
     jobs = [(h, i) for h in range(heads) for i in range(2)]
-    kv_own = kv_all[grp]
+
+    def heads_of(which, j):
+        packed = kv_all[which, j]
+        return jnp.concatenate([packed[:, :kvc], packed[:, kvc:]], axis=0)
+
+    k_own, v_own = heads_of(0, grp), heads_of(1, grp)
     carried = []
     for h, i in jobs:
         size = (i + 1) * qb
-        kb, vb = kv_own[:size, :kvc], kv_own[:size, kvc:]
+        kb, vb = k_own[:size], v_own[:size]
         fade_row = fc_ref[inner, pl.ds(mem * heads + h, 1), pl.ds(pl.multiple_of(grp * gp, gp), size)]
         mask = i * qb + lax.broadcasted_iota(jnp.int32, (qb, size), 0) >= lax.broadcasted_iota(jnp.int32, (qb, size), 1)
         start = (jnp.full((qb, 1), -1e30, F32), jnp.zeros((qb, 1), F32), jnp.zeros((qb, head_dim), F32))
         carried.append(attend(start, queries[h][i * qb : size], kb, vb, fade_row, mask))
 
-    forward(3)
-    earlier(kv_copy)
+    forward(3, range(no - 1, no))
+    for d in range(1, ng):
+        @pl.when(grp >= d)
+        def _(d=d):
+            who = lax.rem(grp + ng - d, ng)
+            kv_copy(d, who).wait_recv()
+            kv_pair(d, mem, who).start()
+
+    for d in range(1, ng):
+        @pl.when(grp >= d)
+        def _(d=d):
+            kv_pair(d, omem, lax.rem(grp + ng - d, ng)).wait_recv()
+
 
     def step(j, carried):
         result = []
-        kb, vb = kv_all[j, :, :kvc], kv_all[j, :, kvc:]
+        kb, vb = heads_of(0, j), heads_of(1, j)
         for (h, i), state_of in zip(jobs, carried):
             fade_row = fc_ref[inner, pl.ds(mem * heads + h, 1), pl.ds(pl.multiple_of(j * gp, gp), gp)]
             result.append(attend(state_of, queries[h][i * qb : (i + 1) * qb], kb, vb, fade_row, None))
@@ -370,13 +404,19 @@
 
     hand_out(0, jnp.concatenate(columns, axis=1) * ag_ref[:, my_half])
 
+    @pl.when(grp > 0)
+    def _():
+        halo_copy.wait_recv()
+        halo[1] = halo[2]
+        recur()
+
     earlier(state_copy)
 
     def enter(j, e):
         return st_all[j, pl.ds(0, 1), :] * e + st_all[j, pl.ds(1, 1), :]
 
     entering = lax.fori_loop(0, grp, enter, jnp.zeros((1, half), F32))
-    whole_state = state + decay * entering
+    whole_state = scanned[1] + scanned[0] * entering
     finish(3)
     gated = whole_state * gelu(dot(normed(), gw[...]))
     hand_out(1, group_rms(gated, rg_ref[:, my_half], lb))
@@ -430,6 +470,12 @@
         for d in range(nto):
             to_core_x(k, d).wait_send()
     later(kv_copy, lambda c: c.wait_send())
+    kv_pair(0, mem, grp).wait_send()
+    for d in range(1, ng):
+        @pl.when(grp >= d)
+        def _(d=d):
+            kv_pair(d, mem, lax.rem(grp + ng - d, ng)).wait_send()
+
     later(state_copy, lambda c: c.wait_send())
 
     @pl.when(grp + 1 < ng)
@@ -472,11 +518,13 @@
         scratch_shapes=[
             pltpu.VMEM((4, span, width), BF16),
             pltpu.VMEM((span, width // nt), BF16),
-            pltpu.VMEM((2 * kvc, width) if flip else (width, 2 * kvc), BF16),
+            pltpu.VMEM((2, *kv_weights[0].shape), BF16),
+            pltpu.VMEM((kvc, width) if flip else (width, kvc), BF16),
             pltpu.VMEM((width, half), BF16),
             pltpu.VMEM((width, half), BF16),
             pltpu.VMEM((width, half), BF16),
-            pltpu.VMEM((ng, 4 * span, 2 * kvc), BF16),
+            pltpu.VMEM((2, ng, 2 * span, 2 * kvc), BF16),
+            pltpu.VMEM((2, 4 * span, half), F32),
             pltpu.VMEM((4, span, half), F32),
             pltpu.VMEM((4 * span + 8, half), F32),
             pltpu.VMEM((3, 8, half), F32),
@@ -488,7 +536,7 @@
             pltpu.VMEM((nto, rows, cols), BF16),
             dma((4, no)), dma((4, no)), dma((4, no)), dma((4, no)),
             dma, dma, dma((2,)), dma((2,)), dma((3, nto)), dma((3, nto)), dma((3, nto)), dma((3, nto)),
-            dma((3,)), dma((3,)), dma((ng,)), dma((ng,)), dma, dma, dma((ng,)), dma((ng,)),
+            dma((3,)), dma((3,)), dma((ng,)), dma((ng,)), dma((ng,)), dma((ng,)), dma, dma, dma((ng,)), dma((ng,)),
             dma((2, 3)), dma((2, 3)), dma((nto,)), dma((nto,)), dma((nto,)), dma((nto,)),
         ],
         compiler_params=pltpu.CompilerParams(

time: 73 us -> 61.9 us (0.85)
  Pallas kernels: 70.6 us -> 59.7 us
    pallas_call x1, Pallas kernels: 70.6 us -> 59.7 us  [body(): pl.pallas_call(functools.partial(kernel, (n, nt, span, head_dim, flip)),...]
where the time goes in v2:
time: 61.9 us; the launch traced here: 61.4 us
  Pallas kernels  59.7 us (96%)
  local copies, waits for them, and re-layouts  1.67 us (3%)
    pallas_call x1, Pallas kernels, body(): pl.pallas_call(functools.partial(kernel, (n, nt, span, head_dim, flip)),...  59.7 us
    unnamed x1, local copies, waits for them, and re-layouts  1.67 us

profile of v2, /device:TPU:1, one launch (start us, length us, event | category | flops | bytes accessed | tf_op | source)
XLA Modules:
  0.0 61.4 jit_solution(14538756294956857746)
XLA Ops:
  0.0 59.7 %shard_map.181 = bf16[256,512]{1,0:T(8,128)(2,1)} custom-call(bf16[256,2048]{1,0:T(8,128)(2,1)} %bitcast.11, f32[1,2048]{1,0:T(1,128)} %bitcast.16, bf16[256,256]{1,0:T(8,128)(2,1)} %wq_ref.1, bf16[64,256]{1,0:T(8,128)(2,1)} %bitcast.14, bf16[64,256]{1,0:T(8,128)(2,1)} %bitcast.15, f32[1,64]{1,0:T(1,128)} %bitcast.20, f32[1,64]{1,0:T(1,128)} %bitcast.21, ...), custom_call_target="tpu_custom_call" | custom-call | tf_op jit(solution)/shard_map/pallas_call | solution.py:513
  59.7 1.7 %copy.21 = bf16[2,128,512]{2,1,0:T(8,128)(2,1)} copy(bf16[2,128,512]{2,1,0:T(8,128)(2,1)} %bitcast.12) | data formatting | bytes 524288

commit v3 on v2

--- a/solution.py
+++ b/solution.py
@@ -14,13 +14,14 @@
 MESH = pl.DeviceIdType.MESH
 
 
-def group_rms(values, gain, width):
-    parts = []
+def group_rms(values, width):
+    lane = lax.broadcasted_iota(jnp.int32, values.shape, 1)
+    squares, scale = values * values, 0.0
     for start in range(0, values.shape[1], width):
-        part = values[:, start : start + width]
-        scale = lax.rsqrt(jnp.mean(part * part, axis=-1, keepdims=True) + EPS)
-        parts.append(part * scale)
-    return jnp.concatenate(parts, axis=1) * gain
+        inside = (lane >= start) & (lane < start + width)
+        mean = jnp.sum(jnp.where(inside, squares, 0.0), axis=-1, keepdims=True) * (1.0 / width)
+        scale = jnp.where(inside, lax.rsqrt(mean + EPS), scale)
+    return values * scale
 
 
 def one_minus_exp(y):
@@ -52,12 +53,12 @@
 
 def kernel(
     dims,
-    x_ref, norm_ref, wq_ref, wk_ref, wv_ref, qg_ref, kg_ref, fc_ref, wr_ref, wg_ref, cw_ref,
-    dgw_ref, igw_ref, dp_ref, de_ref, ag_ref, rg_ref, oa_ref, or_ref,
+    x_any, norm_ref, wq_any, wk_any, wv_any, qg_ref, kg_ref, fc_ref, wr_any, wg_any, cw_ref,
+    dgw_ref, igw_ref, dp_ref, de_any, ag_ref, rg_ref, oa_any, or_any,
     out_ref,
-    xall, xsend, kvsrc, kvw, rw, qw, gw, kv_all, scanned, deg, rin, halo, st_all, act, halves, sums, parts, got,
+    x_ref, wq_ref, wr_ref, wg_ref, de_ref, wall, loads, xall, xsend, kvsrc, kvw, rw, qw, gw, kv_all, scanned, deg, rin, halo, st_all, act, gath, acc,
     zs, zr, fs, fr, xas, xar, xbs, xbr, xcs, xcr, xds, xdr, des, der, kvs, kvr, kps, kpr, hs, hr, ss, sr,
-    acs, acr, ps, pr, qs, qr,
+    acs, acr, ps, pr, qs, qr, ws, wr,
 ):
     n, nt, span, head_dim, flip = dims
     no, nto, ng = n // 2, nt // 2, n // 4
@@ -72,7 +73,7 @@
     touter, tinner = lax.div(tme, 2), lax.rem(tme, 2)
     tmate = touter * 2 + (1 - tinner)
     kr, channels = wq_ref.shape
-    kvc = wk_ref.shape[0 if flip else 1]
+    kvc = wk_any.shape[0 if flip else 1]
     width = x_ref.shape[1]
     half = channels // 2
     quarter = width // nt
@@ -96,6 +97,16 @@
             src_ref=src, dst_ref=dst, send_sem=send, recv_sem=recv, device_id=where, device_id_type=MESH
         )
 
+    out_cols = rows_of(tme, out_ref.shape[1])
+    staged = [
+        pltpu.make_async_copy(src, dst, loads.at[i])
+        for i, (src, dst) in enumerate((
+            (x_any, x_ref), (wk_any, kvsrc.at[0]), (wv_any, kvsrc.at[1]), (wr_any, wr_ref), (wq_any, wq_ref),
+            (wg_any, wg_ref), (de_any, de_ref), (oa_any.at[:, out_cols], wall.at[0, tme]), (or_any.at[:, out_cols], wall.at[1, tme]),
+        ))
+    ]
+    for load in staged:
+        load.start()
     barrier = pltpu.get_barrier_semaphore()
     for d in range(1, n):
         pl.semaphore_signal(barrier, inc=1, device_id={"sp": lax.rem(me + d, n)}, device_id_type=MESH)
@@ -107,8 +118,7 @@
     my_half, my_rows = rows_of(mem, half), rows_of(me, kr)
     my_cols = rows_of(tme, quarter)
 
-    kvsrc[0] = wk_ref[...]
-    kvsrc[1] = wv_ref[...]
+    staged[0].wait()
 
     def scale_rows(seq):
         x = x_ref[rows_of(seq, span), :].astype(F32)
@@ -118,6 +128,8 @@
         x_ref[rows_of(opp, span), my_cols].astype(F32) * scale_rows(opp) * norm_ref[:, my_cols]
     ).astype(BF16)
     xall[mine_block] = (x_ref[rows_of(inner, span), :].astype(F32) * scale_rows(inner) * norm_ref[...]).astype(BF16)
+    for load in staged[1:]:
+        load.wait()
     pl.semaphore_wait(barrier, n - 1 + nt - 1)
 
     weights = (None, wr_ref, wq_ref, wg_ref)
@@ -191,11 +203,14 @@
         src = de_ref.at[rows_of(seq, span), rows_of(member, half)]
         return copy(src, deg.at[mine_block], des.at[i], der.at[i], sp=to)
 
+    def out_weights(a, d, arriving=False):
+        to, who = lax.rem(tme + d, nt), lax.rem(tme + nt - d, nt) if arriving else tme
+        src = wall.at[a, who] if arriving else (oa_any, or_any)[a].at[:, rows_of(to, out_ref.shape[1])]
+        return copy(src, wall.at[a, who], ws.at[a, d - 1], wr.at[a, d - 1], tp=to)
+
     to_mate_x.start()
     to_pair_x[0].start()
     send_z(0)
-    for c in range(3):
-        send_y(c)
     deg[mine_block] = de_ref[rows_of(inner, span), my_half]
     if flip:
         kvw[:, my_rows] = kvsrc[mem]
@@ -208,21 +223,30 @@
     to_mate_x.wait_recv()
     to_pair_x[1].start()
     spread(0)
-    send_z(1)
+    send_y(0)
+    send_y(1)
     to_pair_x[0].wait_recv()
     spread(1)
-    forward(0)
+    forward(0, (1,))
+    send_y(2)
     send_y(3)
     to_pair_x[1].wait_recv()
     spread(2)
+    for a in range(2):
+        for d in range(1, nt):
+            out_weights(a, d).start()
+    send_z(1)
     send_z(2)
+    forward(0, range(2, no))
+    forward(1, (1,))
     for i in range(3):
         extra(i).start()
-    forward(1)
+    forward(1, range(2, no - 1))
     for k in range(3):
         for d in range(1, nto):
             to_far_x(k, d).wait_recv()
             to_core_x(k, d).start()
+    forward(1, (no - 1,))
     for k in range(3):
         for d in range(nto):
             to_core_x(k, d).wait_recv()
@@ -232,7 +256,7 @@
         return xall[...].reshape(gp, width)
 
     kv = lax.dot_general(normed(), kvw[...], (((1,), (1 if flip else 0,)), ((), ())), preferred_element_type=F32)
-    kv = jnp.where(mem == 0, group_rms(kv, kg_ref[...], head_dim), kv).astype(BF16)
+    kv = jnp.where(mem == 0, group_rms(kv, head_dim) * kg_ref[...], kv).astype(BF16)
     kv_all[mem, grp] = jnp.concatenate([kv[: gp // 2], kv[gp // 2 :]], axis=1)
 
     def kv_copy(d, who):
@@ -261,6 +285,8 @@
 
     kv_pair(0, mem, grp).start()
     later(kv_copy, lambda c: c.start())
+    send_z(3)
+    forward(2, range(1, no - 1))
 
     finish(1)
     rec = dot(normed(), rw[...]).astype(BF16).astype(F32)
@@ -273,8 +299,6 @@
     def _():
         halo_copy.start()
 
-    send_z(3)
-    forward(2)
     lb = dgw_ref.shape[1]
 
     def recur():
@@ -311,19 +335,26 @@
         st_all[grp, pl.ds(1, 1), :] = state[gp - 1 : gp]
         later(state_copy, lambda c: c.start())
 
+    forward(2, (no - 1,))
     @pl.when(grp == 0)
     def _():
         recur()
 
+    for d in range(1, ng):
+        @pl.when(grp >= d)
+        def _(d=d):
+            who = lax.rem(grp + ng - d, ng)
+            kv_copy(d, who).wait_recv()
+            kv_pair(d, mem, who).start()
+
+    forward(3, range(1, 2))
     finish(2)
     scaling = head_dim ** (-0.5)
     query = dot(normed(), qw[...])
-    queries = [
-        (group_rms(query[:, h * head_dim : (h + 1) * head_dim], qg_ref[...], head_dim).astype(BF16) * scaling).astype(BF16)
-        for h in range(heads)
-    ]
-
-    forward(3, range(1, no - 1))
+    gains = jnp.concatenate([qg_ref[...]] * heads, axis=1)
+    query = ((group_rms(query, head_dim) * gains).astype(BF16) * scaling).astype(BF16)
+
+    forward(3, range(2, no))
     kv_pair(0, omem, grp).wait_recv()
     def attend(carried, q, kb, vb, fade_row, mask):
         top, total, accum = carried
@@ -343,66 +374,58 @@
         packed = kv_all[which, j]
         return jnp.concatenate([packed[:, :kvc], packed[:, kvc:]], axis=0)
 
-    k_own, v_own = heads_of(0, grp), heads_of(1, grp)
+    def keys_of(j):
+        k = heads_of(0, j)
+        zero = jnp.zeros_like(k)
+        return [jnp.concatenate([k if x == h else zero for x in range(heads)], axis=1) for h in range(heads)]
+
+    k_own, v_own = keys_of(grp), heads_of(1, grp)
     carried = []
     for h, i in jobs:
         size = (i + 1) * qb
-        kb, vb = k_own[:size], v_own[:size]
+        kb, vb = k_own[h][:size], v_own[:size]
         fade_row = fc_ref[inner, pl.ds(mem * heads + h, 1), pl.ds(pl.multiple_of(grp * gp, gp), size)]
         mask = i * qb + lax.broadcasted_iota(jnp.int32, (qb, size), 0) >= lax.broadcasted_iota(jnp.int32, (qb, size), 1)
         start = (jnp.full((qb, 1), -1e30, F32), jnp.zeros((qb, 1), F32), jnp.zeros((qb, head_dim), F32))
-        carried.append(attend(start, queries[h][i * qb : size], kb, vb, fade_row, mask))
-
-    forward(3, range(no - 1, no))
-    for d in range(1, ng):
-        @pl.when(grp >= d)
-        def _(d=d):
-            who = lax.rem(grp + ng - d, ng)
-            kv_copy(d, who).wait_recv()
-            kv_pair(d, mem, who).start()
+        carried.append(attend(start, query[i * qb : size], kb, vb, fade_row, mask))
 
     for d in range(1, ng):
         @pl.when(grp >= d)
         def _(d=d):
             kv_pair(d, omem, lax.rem(grp + ng - d, ng)).wait_recv()
 
-
     def step(j, carried):
         result = []
-        kb, vb = heads_of(0, j), heads_of(1, j)
+        keys, vb = keys_of(j), heads_of(1, j)
         for (h, i), state_of in zip(jobs, carried):
             fade_row = fc_ref[inner, pl.ds(mem * heads + h, 1), pl.ds(pl.multiple_of(j * gp, gp), gp)]
-            result.append(attend(state_of, queries[h][i * qb : (i + 1) * qb], kb, vb, fade_row, None))
+            result.append(attend(state_of, query[i * qb : (i + 1) * qb], keys[h], vb, fade_row, None))
         return tuple(result)
 
     carried = lax.fori_loop(0, grp, step, tuple(carried))
     columns = []
     for h in range(heads):
-        pieces = []
-        for (hh, i), (top, total, accum) in zip(jobs, carried):
-            if hh == h:
-                value = accum / total
-                pieces.append(value * lax.rsqrt(jnp.mean(value * value, axis=-1, keepdims=True) + EPS))
-        columns.append(jnp.concatenate(pieces, axis=0))
+        columns.append(jnp.concatenate([c[2] * (1.0 / c[1]) for (hh, i), c in zip(jobs, carried) if hh == h], axis=0))
+    attended = group_rms(jnp.concatenate(columns, axis=1), head_dim) * ag_ref[:, my_half]
 
     def act_copy(a, i):
         to, block = ((mate, mate_block), (pair, pair_block), (cross, cross_block))[i]
         return copy(
-            act.at[a, block], halves.at[a, rows_of(inner, span), my_half], acs.at[a, i], acr.at[a, i], sp=to
+            act.at[a, block], gath.at[a, tme, rows_of(inner, span), my_half], acs.at[a, i], acr.at[a, i], sp=to
         )
 
     def act_from(a, i):
         seq, member = ((opp, mem), (inner, omem), (opp, omem))[i]
-        ref = halves.at[a, rows_of(seq, span), rows_of(member, half)]
+        ref = gath.at[a, tme, rows_of(seq, span), rows_of(member, half)]
         return copy(ref, ref, acs.at[a, i], acr.at[a, i], sp=mate)
 
     def hand_out(a, values):
         act[a] = values.astype(BF16).reshape(4, span, half)
         for i in range(3):
             act_copy(a, i).start()
-        halves[a, rows_of(inner, span), my_half] = act[a, mine_block]
-
-    hand_out(0, jnp.concatenate(columns, axis=1) * ag_ref[:, my_half])
+        gath[a, tme, rows_of(inner, span), my_half] = act[a, mine_block]
+
+    hand_out(0, attended)
 
     @pl.when(grp > 0)
     def _():
@@ -419,45 +442,60 @@
     whole_state = scanned[1] + scanned[0] * entering
     finish(3)
     gated = whole_state * gelu(dot(normed(), gw[...]))
-    hand_out(1, group_rms(gated, rg_ref[:, my_half], lb))
-    for a in range(2):
+
+    def far_of(d):
+        return lax.rem(touter + nto + d, nto) * 2
+
+    def to_far(a, d):
+        return copy(gath.at[a, tme], gath.at[a, tme], qs.at[a, d - 1], qr.at[a, d - 1], tp=far_of(d) + tinner)
+
+    def to_core(a, d):
+        ref = gath.at[a, far_of(-d) + tinner]
+        return copy(ref, ref, ps.at[a, d], pr.at[a, d], tp=tmate)
+
+    def gather(a):
         for i in range(3):
             act_from(a, i).wait_recv()
-
-    cols = out_ref.shape[1]
-
-    def piece(who):
-        span_cols = pl.ds(pl.multiple_of(who * cols, cols), cols)
-        return dot(halves[0], oa_ref[:, span_cols]) + dot(halves[1], or_ref[:, span_cols])
-
-    def to_mate(s):
-        return pltpu.make_async_remote_copy(
-            src_ref=sums.at[s], dst_ref=parts.at[s], send_sem=ps.at[s], recv_sem=pr.at[s],
-            device_id={"tp": tmate}, device_id_type=MESH,
-        )
-
-    def to_far(d):
-        return pltpu.make_async_remote_copy(
-            src_ref=sums.at[nto + d - 1], dst_ref=got.at[d - 1], send_sem=qs.at[d - 1], recv_sem=qr.at[d - 1],
-            device_id={"tp": lax.rem(touter + d, nto) * 2 + tinner}, device_id_type=MESH,
-        )
-
-    for s in list(range(1, nto)) + [0]:
-        sums[s] = piece(lax.rem(touter + s, nto) * 2 + (1 - tinner)).astype(BF16)
-        to_mate(s).start()
+        for d in range(1, nto):
+            to_far(a, d).start()
+        to_core(a, 0).start()
+
+    def relay(a):
+        for d in range(1, nto):
+            ref = gath.at[a, far_of(-d) + tinner]
+            copy(ref, ref, qs.at[a, d - 1], qr.at[a, d - 1], tp=tmate).wait_recv()
+            to_core(a, d).start()
+
+    def arrive(a, d):
+        ref = gath.at[a, far_of(-d) + 1 - tinner]
+        copy(ref, ref, ps.at[a, d], pr.at[a, d], tp=tmate).wait_recv()
+
+    def term(a, who):
+        return dot(gath[a, who], wall[a, who])
+
+    gather(0)
+    hand_out(1, group_rms(gated, lb) * rg_ref[:, my_half])
+    gather(1)
+    relay(0)
+    for a in range(2):
+        for d in range(1, nt):
+            out_weights(a, d, True).wait_recv()
+    acc[...] = term(0, tme)
+    for d in range(nto):
+        arrive(0, d)
+        acc[...] += term(0, far_of(-d) + 1 - tinner)
+        if d:
+            acc[...] += term(0, far_of(-d) + tinner)
+    acc[...] += term(1, tme)
+    relay(1)
     for d in range(1, nto):
-        mine = piece(lax.rem(touter + d, nto) * 2 + tinner)
-        to_mate(d).wait_recv()
-        sums[nto + d - 1] = (mine + parts[d].astype(F32)).astype(BF16)
-        to_far(d).start()
-    mine = piece(tme)
-    to_mate(0).wait_recv()
-    mine = mine + parts[0].astype(F32)
+        acc[...] += term(1, far_of(-d) + tinner)
+    arrive(1, 0)
+    acc[...] += term(1, tmate)
     for d in range(1, nto):
-        to_far(d).wait_recv()
-        mine = mine + got[d - 1].astype(F32)
-    out_ref[...] = mine.astype(BF16)
-
+        arrive(1, d)
+        acc[...] += term(1, far_of(-d) + 1 - tinner)
+    out_ref[...] = acc[...].astype(BF16)
     for c in range(4):
         drain(c)
     to_mate_x.wait_send()
@@ -485,10 +523,13 @@
     for a in range(2):
         for i in range(3):
             act_copy(a, i).wait_send()
-    for s in range(nto):
-        to_mate(s).wait_send()
-    for d in range(1, nto):
-        to_far(d).wait_send()
+    for a in range(2):
+        for d in range(1, nt):
+            out_weights(a, d).wait_send()
+        for d in range(1, nto):
+            to_far(a, d).wait_send()
+        for d in range(nto):
+            to_core(a, d).wait_send()
 
 
 def body(
@@ -509,13 +550,20 @@
     kv_weights = [w.T if flip else w for w in (key_weight, value_weight)]
     no, nto, ng = n // 2, nt // 2, n // 4
     dma = pltpu.SemaphoreType.DMA
-    vmem = pl.BlockSpec(memory_space=pltpu.VMEM)
+    vmem, far = pl.BlockSpec(memory_space=pltpu.VMEM), pl.BlockSpec(memory_space=pl.ANY)
     out = pl.pallas_call(
         functools.partial(kernel, (n, nt, span, head_dim, flip)),
         out_shape=jax.ShapeDtypeStruct((rows, cols), BF16),
-        in_specs=[vmem] * 19,
+        in_specs=[far if i in (0, 2, 3, 4, 8, 9, 14, 17, 18) else vmem for i in range(19)],
         out_specs=vmem,
         scratch_shapes=[
+            pltpu.VMEM((rows, width), BF16),
+            pltpu.VMEM(query_weight.shape, BF16),
+            pltpu.VMEM(rec_in_weight.shape, BF16),
+            pltpu.VMEM(rec_gate_weight.shape, BF16),
+            pltpu.VMEM((rows, channels), F32),
+            pltpu.VMEM((2, nt, channels, cols), BF16),
+            dma((9,)),
             pltpu.VMEM((4, span, width), BF16),
             pltpu.VMEM((span, width // nt), BF16),
             pltpu.VMEM((2, *kv_weights[0].shape), BF16),
@@ -530,14 +578,13 @@
             pltpu.VMEM((3, 8, half), F32),
             pltpu.VMEM((ng, 8, half), F32),
             pltpu.VMEM((2, 4, span, half), BF16),
-            pltpu.VMEM((2, rows, channels), BF16),
-            pltpu.VMEM((2 * nto, rows, cols), BF16),
-            pltpu.VMEM((nto, rows, cols), BF16),
-            pltpu.VMEM((nto, rows, cols), BF16),
+            pltpu.VMEM((2, nt, rows, channels), BF16),
+            pltpu.VMEM((rows, cols), F32),
             dma((4, no)), dma((4, no)), dma((4, no)), dma((4, no)),
             dma, dma, dma((2,)), dma((2,)), dma((3, nto)), dma((3, nto)), dma((3, nto)), dma((3, nto)),
             dma((3,)), dma((3,)), dma((ng,)), dma((ng,)), dma((ng,)), dma((ng,)), dma, dma, dma((ng,)), dma((ng,)),
-            dma((2, 3)), dma((2, 3)), dma((nto,)), dma((nto,)), dma((nto,)), dma((nto,)),
+            dma((2, 3)), dma((2, 3)), dma((2, nto)), dma((2, nto)), dma((2, nto)), dma((2, nto)),
+            dma((2, nt)), dma((2, nt)),
         ],
         compiler_params=pltpu.CompilerParams(
             collective_id=0, has_side_effects=True, vmem_limit_bytes=60 * 1024 * 1024

time: 61.9 us -> 56.2 us (0.908)
  the two profiles are of different devices: /device:TPU:1 before, /device:TPU:17 now
where the time goes in v3:
time: 56.2 us; the launch traced here: 56 us
  Pallas kernels  54.3 us (97%)
  local copies, waits for them, and re-layouts  1.67 us (3%)
    pallas_call x1, Pallas kernels, body(): pl.pallas_call(functools.partial(kernel, (n, nt, span, head_dim, flip)),...  54.3 us
    unnamed x1, local copies, waits for them, and re-layouts  1.67 us

profile of v3, /device:TPU:17, one launch (start us, length us, event | category | flops | bytes accessed | tf_op | source)
XLA Modules:
  0.0 56.0 jit_solution(10626194283455263143)
XLA Ops:
  0.0 54.3 %shard_map.181 = bf16[256,512]{1,0:T(8,128)(2,1)} custom-call(bf16[256,2048]{1,0:T(8,128)(2,1)} %bitcast.11, f32[1,2048]{1,0:T(1,128)} %bitcast.16, bf16[256,256]{1,0:T(8,128)(2,1)} %wq_any.1, bf16[64,256]{1,0:T(8,128)(2,1)} %bitcast.14, bf16[64,256]{1,0:T(8,128)(2,1)} %bitcast.15, f32[1,64]{1,0:T(1,128)} %bitcast.20, f32[1,64]{1,0:T(1,128)} %bitcast.21, ...), custom_call_target="tpu_custom_call" | custom-call | tf_op jit(solution)/shard_map/pallas_call | solution.py:554
  54.3 1.7 %copy.21 = bf16[2,128,512]{2,1,0:T(8,128)(2,1)} copy(bf16[2,128,512]{2,1,0:T(8,128)(2,1)} %bitcast.12) | data formatting | bytes 524288

commit v4 on v3

--- a/solution.py
+++ b/solution.py
@@ -53,12 +53,13 @@
 
 def kernel(
     dims,
-    x_any, norm_ref, wq_any, wk_any, wv_any, qg_ref, kg_ref, fc_ref, wr_any, wg_any, cw_ref,
-    dgw_ref, igw_ref, dp_ref, de_any, ag_ref, rg_ref, oa_any, or_any,
+    x_any, norm_any, wq_any, wk_any, wv_any, qg_any, kg_any, fc_any, wr_any, wg_any, cw_any,
+    dgw_any, igw_any, dp_any, de_any, ag_any, rg_any, oa_any, or_any,
     out_ref,
-    x_ref, wq_ref, wr_ref, wg_ref, de_ref, wall, loads, xall, xsend, kvsrc, kvw, rw, qw, gw, kv_all, scanned, deg, rin, halo, st_all, act, gath, acc,
-    zs, zr, fs, fr, xas, xar, xbs, xbr, xcs, xcr, xds, xdr, des, der, kvs, kvr, kps, kpr, hs, hr, ss, sr,
-    acs, acr, ps, pr, qs, qr, ws, wr,
+    x_ref, wq_ref, wr_ref, wg_ref, de_ref, wall, norm_ref, qg_ref, kg_ref, fc_ref, cw_ref, dgw_ref, igw_ref, dp_ref,
+    ag_ref, rg_ref, loads, xall, xsend, kvsrc, kvw, rw, qw, gw, kv_all, scanned, deg, rin, halo, st_all, act, gath, acc,
+    zs, zr, fr, xs, xar, xbr, xcr, xdr, des, der, kvs, kvr, kps, kpr, hs, hr, ss, sr,
+    acs, acr, ps, pr, qr, ws, wr,
 ):
     n, nt, span, head_dim, flip = dims
     no, nto, ng = n // 2, nt // 2, n // 4
@@ -101,8 +102,10 @@
     staged = [
         pltpu.make_async_copy(src, dst, loads.at[i])
         for i, (src, dst) in enumerate((
-            (x_any, x_ref), (wk_any, kvsrc.at[0]), (wv_any, kvsrc.at[1]), (wr_any, wr_ref), (wq_any, wq_ref),
+            (x_any, x_ref), (norm_any, norm_ref), (wk_any, kvsrc.at[0]), (wv_any, kvsrc.at[1]), (wr_any, wr_ref), (wq_any, wq_ref),
             (wg_any, wg_ref), (de_any, de_ref), (oa_any.at[:, out_cols], wall.at[0, tme]), (or_any.at[:, out_cols], wall.at[1, tme]),
+            (qg_any, qg_ref), (kg_any, kg_ref), (fc_any, fc_ref), (cw_any, cw_ref), (dgw_any, dgw_ref),
+            (igw_any, igw_ref), (dp_any, dp_ref), (ag_any, ag_ref), (rg_any, rg_ref),
         ))
     ]
     for load in staged:
@@ -119,6 +122,7 @@
     my_cols = rows_of(tme, quarter)
 
     staged[0].wait()
+    staged[1].wait()
 
     def scale_rows(seq):
         x = x_ref[rows_of(seq, span), :].astype(F32)
@@ -128,7 +132,7 @@
         x_ref[rows_of(opp, span), my_cols].astype(F32) * scale_rows(opp) * norm_ref[:, my_cols]
     ).astype(BF16)
     xall[mine_block] = (x_ref[rows_of(inner, span), :].astype(F32) * scale_rows(inner) * norm_ref[...]).astype(BF16)
-    for load in staged[1:]:
+    for load in staged[2:]:
         load.wait()
     pl.semaphore_wait(barrier, n - 1 + nt - 1)
 
@@ -143,18 +147,24 @@
 
     def outward(c, d):
         to = partner(d)
-        return copy(origin(c, lax.rem(to, 2)), place(c, me), zs.at[c, d - 1], zr.at[c, d - 1], sp=to * 2 + inner)
+        return copy(origin(c, lax.rem(to, 2)), place(c, me), zs.at[c], zr.at[c, d - 1], sp=to * 2 + inner)
 
     def inward(c, d):
         who = partner(d) * 2 + inner
-        return copy(place(c, who), place(c, who), zs.at[c, d - 1], zr.at[c, d - 1], sp=mate)
+        return copy(place(c, who), place(c, who), zs.at[c], zr.at[c, d - 1], sp=mate)
 
     def across(c, d, who, src=None):
-        return copy(place(c, who) if src is None else src, place(c, who), fs.at[c, d], fr.at[c, d], sp=mate)
-
-    def send_z(c):
-        for d in range(1, no):
-            outward(c, d).start()
+        return copy(place(c, who) if src is None else src, place(c, who), zs.at[c], fr.at[c], sp=mate)
+
+    line = no == 4
+    middle = (outer == 1) | (outer == 2)
+
+    def send_z(c, which=range(1, no)):
+        for d in which:
+            if line and c > 0 and d == no - 1:
+                pl.when(jnp.logical_not(middle))(outward(c, d).start)
+            else:
+                outward(c, d).start()
 
     def send_y(c):
         across(c, 0, me, origin(c, mem)).start()
@@ -164,34 +174,32 @@
             inward(c, d).wait_recv()
             across(c, d, partner(d) * 2 + inner).start()
 
+    def span_of(c, parts):
+        return kvw.at[:, pl.ds(0, parts * kr)] if c == 0 and flip else buffers[c].at[pl.ds(0, parts * kr), :]
+
     def finish(c):
-        for d in range(no):
-            across(c, d, partner(d) * 2 + opp).wait_recv()
+        copy(span_of(c, no), span_of(c, no), zs.at[c], fr.at[c], sp=mate).wait_recv()
 
     def drain(c):
-        for d in range(1, no):
-            outward(c, d).wait_send()
-        across(c, 0, me, origin(c, mem)).wait_send()
-        for d in range(1, no):
-            across(c, d, partner(d) * 2 + inner).wait_send()
+        copy(span_of(c, n - 1), span_of(c, n - 1), zs.at[c], fr.at[c], sp=mate).wait_send()
 
     def piece_of(block, who=None):
         return xall.at[block, :, my_cols if who is None else rows_of(who, quarter)]
 
-    to_mate_x = copy(xsend, piece_of(mine_block), xas, xar, sp=mate)
+    to_mate_x = copy(xsend, piece_of(mine_block), xs, xar, sp=mate)
     to_pair_x = [
-        copy(piece_of(mine_block), piece_of(mine_block), xbs.at[0], xbr.at[0], sp=pair),
-        copy(piece_of(mate_block), piece_of(mate_block), xbs.at[1], xbr.at[1], sp=pair),
+        copy(piece_of(mine_block), piece_of(mine_block), xs, xbr.at[0], sp=pair),
+        copy(piece_of(mate_block), piece_of(mate_block), xs, xbr.at[1], sp=pair),
     ]
     shared = (mate_block, pair_block, cross_block)
 
     def to_far_x(k, d):
         far = lax.rem(touter + d, nto) * 2 + tinner
-        return copy(piece_of(shared[k]), piece_of(shared[k]), xcs.at[k, d - 1], xcr.at[k, d - 1], tp=far)
+        return copy(piece_of(shared[k]), piece_of(shared[k]), xs, xcr.at[k, d - 1], tp=far)
 
     def to_core_x(k, d):
         ref = piece_of(shared[k], lax.rem(touter + nto - d, nto) * 2 + tinner)
-        return copy(ref, ref, xds.at[k, d], xdr.at[k, d], tp=tmate)
+        return copy(ref, ref, xs, xdr, tp=tmate)
 
     def spread(k):
         for d in range(1, nto):
@@ -201,16 +209,19 @@
     def extra(i):
         to, seq, member = ((mate, opp, mem), (pair, inner, omem), (cross, opp, omem))[i]
         src = de_ref.at[rows_of(seq, span), rows_of(member, half)]
-        return copy(src, deg.at[mine_block], des.at[i], der.at[i], sp=to)
-
-    def out_weights(a, d, arriving=False):
-        to, who = lax.rem(tme + d, nt), lax.rem(tme + nt - d, nt) if arriving else tme
-        src = wall.at[a, who] if arriving else (oa_any, or_any)[a].at[:, rows_of(to, out_ref.shape[1])]
-        return copy(src, wall.at[a, who], ws.at[a, d - 1], wr.at[a, d - 1], tp=to)
+        return copy(src, deg.at[mine_block], des, der, sp=to)
+
+    def out_weights(a, d):
+        to = lax.rem(tme + d, nt)
+        src = (oa_any, or_any)[a].at[:, rows_of(to, out_ref.shape[1])]
+        return copy(src, wall.at[a, tme], ws, wr, tp=to)
 
     to_mate_x.start()
     to_pair_x[0].start()
     send_z(0)
+    if line:
+        for c in range(1, 4):
+            pl.when(middle)(outward(c, no - 1).start)
     deg[mine_block] = de_ref[rows_of(inner, span), my_half]
     if flip:
         kvw[:, my_rows] = kvsrc[mem]
@@ -247,9 +258,8 @@
             to_far_x(k, d).wait_recv()
             to_core_x(k, d).start()
     forward(1, (no - 1,))
-    for k in range(3):
-        for d in range(nto):
-            to_core_x(k, d).wait_recv()
+    shares = xall.at[pl.ds(0, 3), :, pl.ds(0, nto * quarter)]
+    copy(shares, shares, xs, xdr, tp=tmate).wait_recv()
     finish(0)
 
     def normed():
@@ -285,7 +295,7 @@
 
     kv_pair(0, mem, grp).start()
     later(kv_copy, lambda c: c.start())
-    send_z(3)
+    send_z(3, (1,))
     forward(2, range(1, no - 1))
 
     finish(1)
@@ -299,11 +309,11 @@
     def _():
         halo_copy.start()
 
+    send_z(3, range(2, no))
     lb = dgw_ref.shape[1]
 
     def recur():
-        for i, block in ((0, mate_block), (1, pair_block), (2, cross_block)):
-            copy(deg.at[block], deg.at[block], des.at[i], der.at[i], sp=mate).wait_recv()
+        copy(deg.at[pl.ds(0, 3)], deg.at[pl.ds(0, 3)], des, der, sp=mate).wait_recv()
         rin[pl.ds(0, 8), :] = halo[1]
         cw = cw_ref[:, my_half].astype(F32)
         conv = jnp.zeros((gp, half), F32)
@@ -336,10 +346,6 @@
         later(state_copy, lambda c: c.start())
 
     forward(2, (no - 1,))
-    @pl.when(grp == 0)
-    def _():
-        recur()
-
     for d in range(1, ng):
         @pl.when(grp >= d)
         def _(d=d):
@@ -347,14 +353,19 @@
             kv_copy(d, who).wait_recv()
             kv_pair(d, mem, who).start()
 
-    forward(3, range(1, 2))
+    @pl.when(grp > 0)
+    def _():
+        halo_copy.wait_recv()
+        halo[1] = halo[2]
+
+    recur()
     finish(2)
     scaling = head_dim ** (-0.5)
     query = dot(normed(), qw[...])
     gains = jnp.concatenate([qg_ref[...]] * heads, axis=1)
     query = ((group_rms(query, head_dim) * gains).astype(BF16) * scaling).astype(BF16)
 
-    forward(3, range(2, no))
+    forward(3, (1,))
     kv_pair(0, omem, grp).wait_recv()
     def attend(carried, q, kb, vb, fade_row, mask):
         top, total, accum = carried
@@ -389,6 +400,7 @@
         start = (jnp.full((qb, 1), -1e30, F32), jnp.zeros((qb, 1), F32), jnp.zeros((qb, head_dim), F32))
         carried.append(attend(start, query[i * qb : size], kb, vb, fade_row, mask))
 
+    forward(3, range(2, no))
     for d in range(1, ng):
         @pl.when(grp >= d)
         def _(d=d):
@@ -411,13 +423,11 @@
     def act_copy(a, i):
         to, block = ((mate, mate_block), (pair, pair_block), (cross, cross_block))[i]
         return copy(
-            act.at[a, block], gath.at[a, tme, rows_of(inner, span), my_half], acs.at[a, i], acr.at[a, i], sp=to
+            act.at[a, block], gath.at[a, tme, rows_of(inner, span), my_half], acs, acr.at[a], sp=to
         )
 
-    def act_from(a, i):
-        seq, member = ((opp, mem), (inner, omem), (opp, omem))[i]
-        ref = gath.at[a, tme, rows_of(seq, span), rows_of(member, half)]
-        return copy(ref, ref, acs.at[a, i], acr.at[a, i], sp=mate)
+    def act_from(a):
+        copy(act.at[a, pl.ds(0, 3)], act.at[a, pl.ds(0, 3)], acs, acr.at[a], sp=mate).wait_recv()
 
     def hand_out(a, values):
         act[a] = values.astype(BF16).reshape(4, span, half)
@@ -427,12 +437,6 @@
 
     hand_out(0, attended)
 
-    @pl.when(grp > 0)
-    def _():
-        halo_copy.wait_recv()
-        halo[1] = halo[2]
-        recur()
-
     earlier(state_copy)
 
     def enter(j, e):
@@ -447,15 +451,14 @@
         return lax.rem(touter + nto + d, nto) * 2
 
     def to_far(a, d):
-        return copy(gath.at[a, tme], gath.at[a, tme], qs.at[a, d - 1], qr.at[a, d - 1], tp=far_of(d) + tinner)
+        return copy(gath.at[a, tme], gath.at[a, tme], ps, qr.at[a, d - 1], tp=far_of(d) + tinner)
 
     def to_core(a, d):
         ref = gath.at[a, far_of(-d) + tinner]
-        return copy(ref, ref, ps.at[a, d], pr.at[a, d], tp=tmate)
+        return copy(ref, ref, ps, pr.at[a, d], tp=tmate)
 
     def gather(a):
-        for i in range(3):
-            act_from(a, i).wait_recv()
+        act_from(a)
         for d in range(1, nto):
             to_far(a, d).start()
         to_core(a, 0).start()
@@ -463,23 +466,21 @@
     def relay(a):
         for d in range(1, nto):
             ref = gath.at[a, far_of(-d) + tinner]
-            copy(ref, ref, qs.at[a, d - 1], qr.at[a, d - 1], tp=tmate).wait_recv()
+            copy(ref, ref, ps, qr.at[a, d - 1], tp=tmate).wait_recv()
             to_core(a, d).start()
 
     def arrive(a, d):
         ref = gath.at[a, far_of(-d) + 1 - tinner]
-        copy(ref, ref, ps.at[a, d], pr.at[a, d], tp=tmate).wait_recv()
+        copy(ref, ref, ps, pr.at[a, d], tp=tmate).wait_recv()
 
     def term(a, who):
         return dot(gath[a, who], wall[a, who])
 
+    hand_out(1, group_rms(gated, lb) * rg_ref[:, my_half])
     gather(0)
-    hand_out(1, group_rms(gated, lb) * rg_ref[:, my_half])
     gather(1)
     relay(0)
-    for a in range(2):
-        for d in range(1, nt):
-            out_weights(a, d, True).wait_recv()
+    copy(wall.at[:, pl.ds(0, nt - 1)], wall.at[:, pl.ds(0, nt - 1)], ws, wr, tp=tmate).wait_recv()
     acc[...] = term(0, tme)
     for d in range(nto):
         arrive(0, d)
@@ -498,15 +499,8 @@
     out_ref[...] = acc[...].astype(BF16)
     for c in range(4):
         drain(c)
-    to_mate_x.wait_send()
-    for c in to_pair_x:
-        c.wait_send()
-    for k in range(3):
-        extra(k).wait_send()
-        for d in range(1, nto):
-            to_far_x(k, d).wait_send()
-        for d in range(nto):
-            to_core_x(k, d).wait_send()
+    copy(xall.at[pl.ds(0, 3)], xall.at[pl.ds(0, 3)], xs, xar, sp=mate).wait_send()
+    copy(deg.at[pl.ds(0, 3)], deg.at[pl.ds(0, 3)], des, der, sp=mate).wait_send()
     later(kv_copy, lambda c: c.wait_send())
     kv_pair(0, mem, grp).wait_send()
     for d in range(1, ng):
@@ -520,16 +514,9 @@
     def _():
         halo_copy.wait_send()
 
-    for a in range(2):
-        for i in range(3):
-            act_copy(a, i).wait_send()
-    for a in range(2):
-        for d in range(1, nt):
-            out_weights(a, d).wait_send()
-        for d in range(1, nto):
-            to_far(a, d).wait_send()
-        for d in range(nto):
-            to_core(a, d).wait_send()
+    copy(act.at[:, pl.ds(0, 3)], act.at[:, pl.ds(0, 3)], acs, acr.at[0], sp=mate).wait_send()
+    copy(wall.at[:, pl.ds(0, nt - 1)], wall.at[:, pl.ds(0, nt - 1)], ws, wr, tp=tmate).wait_send()
+    copy(gath.at[:, pl.ds(0, nt - 1)], gath.at[:, pl.ds(0, nt - 1)], ps, wr, tp=tmate).wait_send()
 
 
 def body(
@@ -550,11 +537,11 @@
     kv_weights = [w.T if flip else w for w in (key_weight, value_weight)]
     no, nto, ng = n // 2, nt // 2, n // 4
     dma = pltpu.SemaphoreType.DMA
-    vmem, far = pl.BlockSpec(memory_space=pltpu.VMEM), pl.BlockSpec(memory_space=pl.ANY)
+    vmem, far = pl.BlockSpec(memory_space=pltpu.VMEM), pl.BlockSpec(memory_space=pltpu.HBM)
     out = pl.pallas_call(
         functools.partial(kernel, (n, nt, span, head_dim, flip)),
-        out_shape=jax.ShapeDtypeStruct((rows, cols), BF16),
-        in_specs=[far if i in (0, 2, 3, 4, 8, 9, 14, 17, 18) else vmem for i in range(19)],
+        out_shape=pltpu.VMEM((rows, cols), BF16),
+        in_specs=[far] * 19,
         out_specs=vmem,
         scratch_shapes=[
             pltpu.VMEM((rows, width), BF16),
@@ -563,7 +550,17 @@
             pltpu.VMEM(rec_gate_weight.shape, BF16),
             pltpu.VMEM((rows, channels), F32),
             pltpu.VMEM((2, nt, channels, cols), BF16),
-            dma((9,)),
+            pltpu.VMEM((1, width), F32),
+            pltpu.VMEM((1, head_dim), F32),
+            pltpu.VMEM((1, head_dim), F32),
+            pltpu.VMEM(forget_cache.shape, F32),
+            pltpu.VMEM(conv_weight.shape, BF16),
+            pltpu.VMEM(decay_gate_weight.shape, BF16),
+            pltpu.VMEM(input_gate_weight.shape, BF16),
+            pltpu.VMEM((1, channels), F32),
+            pltpu.VMEM((1, qc), F32),
+            pltpu.VMEM((1, channels), F32),
+            dma((19,)),
             pltpu.VMEM((4, span, width), BF16),
             pltpu.VMEM((span, width // nt), BF16),
             pltpu.VMEM((2, *kv_weights[0].shape), BF16),
@@ -580,11 +577,9 @@
             pltpu.VMEM((2, 4, span, half), BF16),
             pltpu.VMEM((2, nt, rows, channels), BF16),
             pltpu.VMEM((rows, cols), F32),
-            dma((4, no)), dma((4, no)), dma((4, no)), dma((4, no)),
-            dma, dma, dma((2,)), dma((2,)), dma((3, nto)), dma((3, nto)), dma((3, nto)), dma((3, nto)),
-            dma((3,)), dma((3,)), dma((ng,)), dma((ng,)), dma((ng,)), dma((ng,)), dma, dma, dma((ng,)), dma((ng,)),
-            dma((2, 3)), dma((2, 3)), dma((2, nto)), dma((2, nto)), dma((2, nto)), dma((2, nto)),
-            dma((2, nt)), dma((2, nt)),
+            dma((4,)), dma((4, no - 1)), dma((4,)), dma, dma, dma((2,)), dma((3, nto - 1)), dma,
+            dma, dma, dma((ng - 1,)), dma((ng - 1,)), dma((ng,)), dma((ng,)), dma, dma, dma((ng - 1,)), dma((ng - 1,)),
+            dma, dma((2,)), dma, dma((2, nto)), dma((2, nto - 1)), dma, dma,
         ],
         compiler_params=pltpu.CompilerParams(
             collective_id=0, has_side_effects=True, vmem_limit_bytes=60 * 1024 * 1024

time: 56.2 us -> 52.2 us (0.929)
  the two profiles are of different devices: /device:TPU:17 before, /device:TPU:1 now
where the time goes in v4:
time: 52.2 us; the launch traced here: 52.1 us
  Pallas kernels  51.4 us (98%)
  local copies, waits for them, and re-layouts  0.71 us (1%)
    pallas_call x1, Pallas kernels, body(): pl.pallas_call(functools.partial(kernel, (n, nt, span, head_dim, flip)),...  51.4 us

profile of v4, /device:TPU:1, one launch (start us, length us, event | category | flops | bytes accessed | tf_op | source)
XLA Modules:
  0.0 52.1 jit_solution(6176732785761339051)
XLA Ops:
  0.0 51.4 %shard_map.181 = bf16[256,512]{1,0:T(8,128)(2,1)S(1)} custom-call(bf16[256,2048]{1,0:T(8,128)(2,1)} %bitcast.12, f32[1,2048]{1,0:T(1,128)} %bitcast.16, bf16[256,256]{1,0:T(8,128)(2,1)} %wq_any.1, bf16[64,256]{1,0:T(8,128)(2,1)} %bitcast.14, bf16[64,256]{1,0:T(8,128)(2,1)} %bitcast.15, f32[1,64]{1,0:T(1,128)} %bitcast.20, f32[1,64]{1,0:T(1,128)} %bitcast.21, ...), custom_call_target="tpu_custom_call" | custom-call | tf_op jit(solution)/shard_map/pallas_call | solution.py:541
  51.4 0.7 %copy.21 = bf16[2,128,512]{2,1,0:T(8,128)(2,1)} copy(bf16[2,128,512]{2,1,0:T(8,128)(2,1)S(1)} %bitcast.11) | data formatting | bytes 524288

commit v5 on v4

--- a/solution.py
+++ b/solution.py
@@ -353,19 +353,33 @@
             kv_copy(d, who).wait_recv()
             kv_pair(d, mem, who).start()
 
+    early = (grp > 0) & (mem == 0)
+    late = (grp > 0) & (mem > 0)
+    @pl.when(early)
+    def _():
+        forward(3, (1,))
+
     @pl.when(grp > 0)
     def _():
         halo_copy.wait_recv()
         halo[1] = halo[2]
 
     recur()
+    @pl.when(grp == 0)
+    def _():
+        forward(3, (1,))
+
     finish(2)
     scaling = head_dim ** (-0.5)
     query = dot(normed(), qw[...])
     gains = jnp.concatenate([qg_ref[...]] * heads, axis=1)
     query = ((group_rms(query, head_dim) * gains).astype(BF16) * scaling).astype(BF16)
 
-    forward(3, (1,))
+    @pl.when(late)
+    def _():
+        forward(3, (1,))
+
+    forward(3, range(2, no))
     kv_pair(0, omem, grp).wait_recv()
     def attend(carried, q, kb, vb, fade_row, mask):
         top, total, accum = carried
@@ -400,7 +414,6 @@
         start = (jnp.full((qb, 1), -1e30, F32), jnp.zeros((qb, 1), F32), jnp.zeros((qb, head_dim), F32))
         carried.append(attend(start, query[i * qb : size], kb, vb, fade_row, mask))
 
-    forward(3, range(2, no))
     for d in range(1, ng):
         @pl.when(grp >= d)
         def _(d=d):
@@ -444,9 +457,6 @@
 
     entering = lax.fori_loop(0, grp, enter, jnp.zeros((1, half), F32))
     whole_state = scanned[1] + scanned[0] * entering
-    finish(3)
-    gated = whole_state * gelu(dot(normed(), gw[...]))
-
     def far_of(d):
         return lax.rem(touter + nto + d, nto) * 2
 
@@ -475,6 +485,9 @@
 
     def term(a, who):
         return dot(gath[a, who], wall[a, who])
+
+    finish(3)
+    gated = whole_state * gelu(dot(normed(), gw[...]))
 
     hand_out(1, group_rms(gated, lb) * rg_ref[:, my_half])
     gather(0)

time: 52.2 us -> 51.3 us (0.983)
  Pallas kernels: 51.4 us -> 50.5 us
    pallas_call x1, Pallas kernels: 51.4 us -> 50.5 us  [body(): pl.pallas_call(functools.partial(kernel, (n, nt, span, head_dim, flip)),...]
where the time goes in v5:
time: 51.3 us; the launch traced here: 51.2 us
  Pallas kernels  50.5 us (98%)
  local copies, waits for them, and re-layouts  0.71 us (1%)
    pallas_call x1, Pallas kernels, body(): pl.pallas_call(functools.partial(kernel, (n, nt, span, head_dim, flip)),...  50.5 us

profile of v5, /device:TPU:1, one launch (start us, length us, event | category | flops | bytes accessed | tf_op | source)
XLA Modules:
  0.0 51.2 jit_solution(11051762418202408350)
XLA Ops:
  0.0 50.5 %shard_map.181 = bf16[256,512]{1,0:T(8,128)(2,1)S(1)} custom-call(bf16[256,2048]{1,0:T(8,128)(2,1)} %bitcast.12, f32[1,2048]{1,0:T(1,128)} %bitcast.16, bf16[256,256]{1,0:T(8,128)(2,1)} %wq_any.1, bf16[64,256]{1,0:T(8,128)(2,1)} %bitcast.14, bf16[64,256]{1,0:T(8,128)(2,1)} %bitcast.15, f32[1,64]{1,0:T(1,128)} %bitcast.20, f32[1,64]{1,0:T(1,128)} %bitcast.21, ...), custom_call_target="tpu_custom_call" | custom-call | tf_op jit(solution)/shard_map/pallas_call | solution.py:554
  50.5 0.7 %copy.21 = bf16[2,128,512]{2,1,0:T(8,128)(2,1)} copy(bf16[2,128,512]{2,1,0:T(8,128)(2,1)S(1)} %bitcast.11) | data formatting | bytes 524288

commit v6 on v5

--- a/solution.py
+++ b/solution.py
@@ -248,10 +248,10 @@
             out_weights(a, d).start()
     send_z(1)
     send_z(2)
+    for i in range(3):
+        extra(i).start()
     forward(0, range(2, no))
     forward(1, (1,))
-    for i in range(3):
-        extra(i).start()
     forward(1, range(2, no - 1))
     for k in range(3):
         for d in range(1, nto):
@@ -269,6 +269,21 @@
     kv = jnp.where(mem == 0, group_rms(kv, head_dim) * kg_ref[...], kv).astype(BF16)
     kv_all[mem, grp] = jnp.concatenate([kv[: gp // 2], kv[gp // 2 :]], axis=1)
 
+    def project_part(weights, line):
+        total = 0.0
+        for z in range(no):
+            block = rows_of(z * 2 + line, kr)
+            total = total + dot(xall[:, :, block].reshape(gp, kr), weights[block, :])
+        return total
+
+    def project(c):
+        if not flip:
+            finish(c)
+            return dot(normed(), buffers[c][...])
+        total = project_part(buffers[c], inner)
+        finish(c)
+        return total + project_part(buffers[c], opp)
+
     def kv_copy(d, who):
         to, ref = lax.rem(grp + d, ng) * 4 + mem * 2 + inner, kv_all.at[mem, who]
         return copy(ref, ref, kvs.at[d - 1], kvr.at[d - 1], sp=to)
@@ -298,8 +313,7 @@
     send_z(3, (1,))
     forward(2, range(1, no - 1))
 
-    finish(1)
-    rec = dot(normed(), rw[...]).astype(BF16).astype(F32)
+    rec = project(1).astype(BF16).astype(F32)
     rin[pl.ds(8, gp), :] = rec
     halo[0] = rec[gp - 8 : gp]
     halo[1] = jnp.zeros_like(halo[1])
@@ -369,9 +383,8 @@
     def _():
         forward(3, (1,))
 
-    finish(2)
+    query = project(2)
     scaling = head_dim ** (-0.5)
-    query = dot(normed(), qw[...])
     gains = jnp.concatenate([qg_ref[...]] * heads, axis=1)
     query = ((group_rms(query, head_dim) * gains).astype(BF16) * scaling).astype(BF16)
 
@@ -486,22 +499,23 @@
     def term(a, who):
         return dot(gath[a, who], wall[a, who])
 
-    finish(3)
-    gated = whole_state * gelu(dot(normed(), gw[...]))
+    gate_proj = project(3)
+    gated = whole_state * gelu(gate_proj)
 
     hand_out(1, group_rms(gated, lb) * rg_ref[:, my_half])
     gather(0)
     gather(1)
     relay(0)
     copy(wall.at[:, pl.ds(0, nt - 1)], wall.at[:, pl.ds(0, nt - 1)], ws, wr, tp=tmate).wait_recv()
-    acc[...] = term(0, tme)
-    for d in range(nto):
+    acc[...] = term(0, tme) + term(1, tme)
+    arrive(0, 0)
+    acc[...] += term(0, tmate)
+    for d in range(1, nto):
+        acc[...] += term(0, far_of(-d) + tinner)
+    relay(1)
+    for d in range(1, nto):
         arrive(0, d)
         acc[...] += term(0, far_of(-d) + 1 - tinner)
-        if d:
-            acc[...] += term(0, far_of(-d) + tinner)
-    acc[...] += term(1, tme)
-    relay(1)
     for d in range(1, nto):
         acc[...] += term(1, far_of(-d) + tinner)
     arrive(1, 0)

time: 51.3 us -> 50.3 us (0.981)
  Pallas kernels: 50.5 us -> 49.5 us
    pallas_call x1, Pallas kernels: 50.5 us -> 49.5 us  [body(): pl.pallas_call(functools.partial(kernel, (n, nt, span, head_dim, flip)),...]
where the time goes in v6:
time: 50.3 us; the launch traced here: 50.2 us
  Pallas kernels  49.5 us (98%)
  local copies, waits for them, and re-layouts  0.71 us (1%)
    pallas_call x1, Pallas kernels, body(): pl.pallas_call(functools.partial(kernel, (n, nt, span, head_dim, flip)),...  49.5 us

profile of v6, /device:TPU:1, one launch (start us, length us, event | category | flops | bytes accessed | tf_op | source)
XLA Modules:
  0.0 50.2 jit_solution(963271676106357215)
XLA Ops:
  0.0 49.5 %shard_map.181 = bf16[256,512]{1,0:T(8,128)(2,1)S(1)} custom-call(bf16[256,2048]{1,0:T(8,128)(2,1)} %bitcast.12, f32[1,2048]{1,0:T(1,128)} %bitcast.16, bf16[256,256]{1,0:T(8,128)(2,1)} %wq_any.1, bf16[64,256]{1,0:T(8,128)(2,1)} %bitcast.14, bf16[64,256]{1,0:T(8,128)(2,1)} %bitcast.15, f32[1,64]{1,0:T(1,128)} %bitcast.20, f32[1,64]{1,0:T(1,128)} %bitcast.21, ...), custom_call_target="tpu_custom_call" | custom-call | tf_op jit(solution)/shard_map/pallas_call | solution.py:568
  49.5 0.7 %copy.21 = bf16[2,128,512]{2,1,0:T(8,128)(2,1)} copy(bf16[2,128,512]{2,1,0:T(8,128)(2,1)S(1)} %bitcast.11) | data formatting | bytes 524288
